TPU v7x, 32 devices: a whole 2x2x4 slice. The times are simulated.
32 devices in a mesh: ep: 4 (over y, x), tp: 8 (over z, core).
Axes of the slice: x: 2, y: 2, z: 4, core: 2. Of those that a mesh axis runs over, the one named last changes fastest.
Arguments:
- tokens: bfloat16 [768, 4096], P('ep', 'tp'), may hold values from -6 to 6
- cotangent: bfloat16 [768, 4096], P('ep', 'tp'), may hold values from -4 to 4
- routes: int32 [768, 2], P('ep'), may hold values from 0 to 7, all different within a row; in each aligned block of 192 rows (0 to 191, 192 to 383, ...) at most 72 rows name the same one
- gate_weights: bfloat16 [768, 2], P('ep'), may hold values from 0.099609375 to 2.5
- expert_gate: bfloat16 [8, 4096, 1024], P('ep', 'tp'), may hold values from -0.09375 to 0.09375
- expert_up: bfloat16 [8, 4096, 1024], P('ep', 'tp'), may hold values from -0.09375 to 0.09375
- expert_down: bfloat16 [8, 4096, 1024], P('ep', 'tp'), may hold values from -0.1875 to 0.1875
- shared_gate: bfloat16 [4096, 1024], P('tp'), may hold values from -0.09375 to 0.09375
- shared_up: bfloat16 [4096, 1024], P('tp'), may hold values from -0.09375 to 0.09375
- shared_down: bfloat16 [4096, 1024], P('tp'), may hold values from -0.1875 to 0.1875
Outputs:
- token_grad: bfloat16 [768, 4096], P('ep', 'tp')
- gate_grad: bfloat16 [768, 2], P('ep')
- expert_grads: bfloat16 [3, 8, 4096, 1024], P(None, 'ep', 'tp')
- shared_grads: float32 [3, 4096, 1024], P(None, 'tp', 'ep')
- expert_norms: float32 [3, 8, 1024], P(None, 'ep')
- shared_norms: float32 [3, 1024], P(None, 'ep')
Inputs may be any that keep to these rules, and one draw needn't show every extreme that they name: `routes`: each row names 2 different experts. In each aligned block of 192 rows no expert is named by more than 72 rows, a bound that some block reaches.
All inputs are finite; a program needn't handle non-finite values.
Results may differ from a plain program's by a relative error of at most 0.0069.
Values may be sent and summed in bfloat16 or wider, within the bound.
A program may use at most 128 MiB of HBM per device.

v0:
```python
import jax
import jax.numpy as jnp
from jax import lax
from jax.sharding import PartitionSpec as P


def row_backward(summed, weights):
    hidden = summed.shape[1] // 3
    pre_gate = summed[:, :hidden]
    pre_up = summed[:, hidden : 2 * hidden]
    back_act = summed[:, 2 * hidden :]
    sigmoid_gate = jax.nn.sigmoid(pre_gate)
    silu_gate = pre_gate * sigmoid_gate
    activation = silu_gate * pre_up
    act_grad = weights[:, None] * back_act
    grad_up = (act_grad * silu_gate).astype(jnp.bfloat16)
    grad_gate = (act_grad * pre_up * sigmoid_gate * (1.0 + pre_gate * (1.0 - sigmoid_gate))).astype(
        jnp.bfloat16
    )
    scaled_act = (weights[:, None] * activation).astype(jnp.bfloat16)
    weight_grad = jnp.sum(activation * back_act, axis=1).astype(jnp.bfloat16)
    return (grad_gate, grad_up, scaled_act, weight_grad)


def body(
    tokens,
    cotangent,
    routes,
    gate_weights,
    expert_gate,
    expert_up,
    expert_down,
    shared_gate,
    shared_up,
    shared_down,
):
    groups = lax.axis_size("ep")
    tp_lanes = lax.axis_size("tp")
    rows_here, feat_width = tokens.shape
    choose = routes.shape[1]
    local_experts = expert_gate.shape[0]
    hidden = expert_gate.shape[2]
    experts = local_experts * groups
    capacity = 3 * rows_here * choose // (2 * experts)
    total_slots = experts * capacity
    flat_expert = routes.reshape(-1)
    onehot = (flat_expert[:, None] == jnp.arange(experts, dtype=jnp.int32)[None, :]).astype(
        jnp.int32
    )
    position = jnp.sum((jnp.cumsum(onehot, axis=0) - onehot) * onehot, axis=1)
    slot_index = flat_expert * capacity + position
    owner_row = jnp.arange(rows_here * choose, dtype=jnp.int32) // choose
    slot_token = jnp.zeros((total_slots,), jnp.int32).at[slot_index].set(owner_row)
    slot_live = (
        jnp.zeros((total_slots,), jnp.bfloat16)
        .at[slot_index]
        .set(jnp.ones((rows_here * choose,), jnp.bfloat16))
    )
    slot_weight = (
        jnp.zeros((total_slots,), jnp.bfloat16).at[slot_index].set(gate_weights.reshape(-1))
    )
    send_tokens = (tokens[slot_token] * slot_live[:, None]).reshape(
        groups, local_experts * capacity, feat_width
    )
    send_cotan = (cotangent[slot_token] * slot_live[:, None]).reshape(
        groups, local_experts * capacity, feat_width
    )
    recv_tokens, recv_cotan, recv_weight = (
        lax.all_to_all(send_tokens, "ep", split_axis=0, concat_axis=0, tiled=True),
        lax.all_to_all(send_cotan, "ep", split_axis=0, concat_axis=0, tiled=True),
        lax.all_to_all(
            slot_weight.reshape(groups, local_experts * capacity),
            "ep",
            split_axis=0,
            concat_axis=0,
            tiled=True,
        ),
    )
    in_tokens = recv_tokens.reshape(groups, local_experts, capacity, feat_width)
    in_cotan = recv_cotan.reshape(groups, local_experts, capacity, feat_width)

    def project(row_block, weight):
        return jnp.einsum(
            "secd,edf->secf", row_block, weight, preferred_element_type=jnp.float32
        ).reshape(total_slots, hidden)

    pre_gate = jnp.concatenate(
        [
            project(in_tokens, expert_gate),
            jnp.dot(tokens, shared_gate, preferred_element_type=jnp.float32),
        ],
        axis=0,
    )
    pre_up = jnp.concatenate(
        [
            project(in_tokens, expert_up),
            jnp.dot(tokens, shared_up, preferred_element_type=jnp.float32),
        ],
        axis=0,
    )
    pre_back = jnp.concatenate(
        [
            project(in_cotan, expert_down),
            jnp.dot(cotangent, shared_down, preferred_element_type=jnp.float32),
        ],
        axis=0,
    )
    partials = jnp.concatenate([pre_gate, pre_up, pre_back], axis=1).astype(jnp.bfloat16)
    all_rows = partials.shape[0]
    piece = all_rows // tp_lanes
    weights = jnp.concatenate(
        [recv_weight.reshape(-1).astype(jnp.float32), jnp.ones((rows_here,), jnp.float32)]
    )
    arrived = lax.all_to_all(
        partials.reshape(tp_lanes, piece, 3 * hidden), "tp", split_axis=0, concat_axis=0, tiled=True
    )
    share = jnp.sum(arrived.astype(jnp.float32), axis=0)
    own_weights = lax.dynamic_slice_in_dim(weights, lax.axis_index("tp") * piece, piece)
    part_gate, part_up, part_scaled, part_weight = row_backward(share, own_weights)
    grad_gate, grad_up, scaled_act, weight_grad = (
        lax.all_gather(part_gate, "tp", axis=0, tiled=True),
        lax.all_gather(part_up, "tp", axis=0, tiled=True),
        lax.all_gather(part_scaled, "tp", axis=0, tiled=True),
        lax.all_gather(part_weight, "tp", axis=0, tiled=True),
    )
    routed_gate = grad_gate[:total_slots].reshape(groups, local_experts, capacity, hidden)
    routed_up = grad_up[:total_slots].reshape(groups, local_experts, capacity, hidden)
    routed_scaled = scaled_act[:total_slots].reshape(groups, local_experts, capacity, hidden)
    slot_grad = (
        jnp.einsum("secf,edf->secd", routed_gate, expert_gate, preferred_element_type=jnp.float32)
        + jnp.einsum("secf,edf->secd", routed_up, expert_up, preferred_element_type=jnp.float32)
    ).astype(jnp.bfloat16)
    back_rows, back_weight = (
        lax.all_to_all(
            slot_grad.reshape(groups, local_experts * capacity, feat_width),
            "ep",
            split_axis=0,
            concat_axis=0,
            tiled=True,
        ),
        lax.all_to_all(
            weight_grad[:total_slots].reshape(groups, local_experts * capacity),
            "ep",
            split_axis=0,
            concat_axis=0,
            tiled=True,
        ),
    )
    routed_sum = jnp.sum(
        back_rows.reshape(total_slots, feat_width)[slot_index]
        .astype(jnp.float32)
        .reshape(rows_here, choose, feat_width),
        axis=1,
    )
    shared_gg = grad_gate[total_slots:]
    shared_gu = grad_up[total_slots:]
    shared_sa = scaled_act[total_slots:]
    shared_part = jnp.einsum(
        "tf,df->td", shared_gg, shared_gate, preferred_element_type=jnp.float32
    ) + jnp.einsum("tf,df->td", shared_gu, shared_up, preferred_element_type=jnp.float32)
    token_grad = (routed_sum + shared_part).astype(jnp.bfloat16)
    gate_grad = back_weight.reshape(-1)[slot_index].reshape(rows_here, choose)
    expert_stack = jnp.stack(
        [
            jnp.einsum(
                "secd,secf->edf", in_tokens, routed_gate, preferred_element_type=jnp.float32
            ),
            jnp.einsum("secd,secf->edf", in_tokens, routed_up, preferred_element_type=jnp.float32),
            jnp.einsum(
                "secd,secf->edf", in_cotan, routed_scaled, preferred_element_type=jnp.float32
            ),
        ]
    )
    shared_stack = jnp.stack(
        [
            jnp.einsum("td,tf->df", tokens, shared_gg, preferred_element_type=jnp.float32),
            jnp.einsum("td,tf->df", tokens, shared_gu, preferred_element_type=jnp.float32),
            jnp.einsum("td,tf->df", cotangent, shared_sa, preferred_element_type=jnp.float32),
        ]
    )
    shared_summed = lax.psum_scatter(shared_stack, "ep", scatter_dimension=2, tiled=True)
    expert_sq = jnp.sum(expert_stack * expert_stack, axis=2)
    shared_sq = jnp.sum(shared_summed * shared_summed, axis=1)
    expert_norms, shared_norms = lax.psum((expert_sq, shared_sq), "tp")
    inverse_width = 1.0 / (feat_width * tp_lanes)
    return (
        token_grad,
        gate_grad,
        expert_stack.astype(jnp.bfloat16),
        shared_summed,
        expert_norms * inverse_width,
        shared_norms * inverse_width,
    )


def solution(mesh):
    return jax.shard_map(
        body,
        mesh=mesh,
        in_specs=(
            P("ep", "tp"),
            P("ep", "tp"),
            P("ep", None),
            P("ep", None),
            P("ep", "tp", None),
            P("ep", "tp", None),
            P("ep", "tp", None),
            P("tp", None),
            P("tp", None),
            P("tp", None),
        ),
        out_specs=(
            P("ep", "tp"),
            P("ep", None),
            P(None, "ep", "tp", None),
            P(None, "tp", "ep"),
            P(None, "ep", None),
            P(None, "ep"),
        ),
        check_vma=False,
    )
```

profile of v0, /device:TPU:0, one launch (start us, length us, event | category | flops | bytes accessed | tf_op | source)
XLA Modules:
  0.0 379.8 jit_solution(4222144061320989681)
XLA Ops:
  10.7 3.0 scatter_custom_fusion.2
  13.8 2.9 scatter_custom_fusion.1
  16.7 2.7 gather_fusion.1
  19.5 3.3 gather_fusion
  22.7 2.2 broadcast_multiply_fusion.1
  25.0 5.2 %all-to-all-start.2 = ((bf16[4,144,512]{2,1,0:T(8,128)(2,1)}), bf16[4,144,512]{2,1,0:T(8,128)(2,1)S(1)}, u32[]{:S(2)}, u32[]{:S(2)}) async-start(bf16[4,144,512]{2,1,0:T(8,128)(2,1)} %get-tuple-element.31), calls=%async_computation.2 | async-start | bytes 1179648 | tf_op jit(solution)/shard_map/all_to_all | solution.py:70
  30.2 2.3 convolution_convert_fusion
  32.5 1.6 convolution_convert_fusion.2
  34.1 4.7 %all-to-all-done.2 = bf16[4,144,512]{2,1,0:T(8,128)(2,1)S(1)} async-done(((bf16[4,144,512]{2,1,0:T(8,128)(2,1)}), bf16[4,144,512]{2,1,0:T(8,128)(2,1)S(1)}, u32[]{:S(2)}, u32[]{:S(2)}) %all-to-all-start.2) | async-done | bytes 589856 | tf_op jit(solution)/shard_map/all_to_all | solution.py:70
  39.7 3.5 all-to-all-start.1
  43.2 2.3 convolution_convert_fusion.1
  45.8 3.0 scatter_custom_fusion
  49.5 2.6 fusion.20
  53.2 4.2 %all-to-all-start = ((bf16[4,1,144]{2,1,0:T(2,128)(2,1)}), bf16[4,1,144]{2,1,0:T(2,128)(2,1)S(1)}, u32[]{:S(2)}, u32[]{:S(2)}) async-start(bf16[4,1,144]{2,1,0:T(2,128)(2,1)} %all_to_all.32), calls=%async_computation | async-start | bytes 8192 | tf_op jit(solution)/shard_map/all_to_all | solution.py:71
  57.3 2.4 fusion.26
  62.4 2.4 pad_maximum_fusion.2
  64.8 4.9 %all-to-all-start.3 = ((bf16[8,96,3072]{2,1,0:T(8,128)(2,1)}), bf16[8,96,3072]{2,1,0:T(8,128)(2,1)}, u32[]{:S(2)}, u32[]{:S(2)}) async-start(bf16[8,96,3072]{2,1,0:T(8,128)(2,1)} %pad_maximum_fusion.2), calls=%async_computation.3 | async-start | bytes 9437184 | tf_op jit(solution)/shard_map/all_to_all | solution.py:114
  69.9 105.1 %all-to-all-done.3 = bf16[8,96,3072]{2,1,0:T(8,128)(2,1)} async-done(((bf16[8,96,3072]{2,1,0:T(8,128)(2,1)}), bf16[8,96,3072]{2,1,0:T(8,128)(2,1)}, u32[]{:S(2)}, u32[]{:S(2)}) %all-to-all-start.3) | async-done | bytes 4718624 | tf_op jit(solution)/shard_map/all_to_all | solution.py:114
  175.0 3.3 convert_reduce_fusion
  178.3 1.2 multiply_convert_fusion
  181.1 23.3 %all-gather.4.cloned.1.call-done = bf16[768,1024]{1,0:T(8,128)(2,1)} async-done(((bf16[96,1024]{1,0:T(8,128)(2,1)}), bf16[768,1024]{1,0:T(8,128)(2,1)}) %all-gather.4.cloned.1.call-update) | async-done | bytes 1572880 | tf_op jit(solution)/shard_map/all_gather | solution.py:121
  204.4 2.8 convolution_bitcast_fusion.5
  207.2 23.8 %all-gather.6.cloned.1.call-done = bf16[768,1024]{1,0:T(8,128)(2,1)} async-done(((bf16[96,1024]{1,0:T(8,128)(2,1)}), bf16[768,1024]{1,0:T(8,128)(2,1)}) %all-gather.6.cloned.1.call-update) | async-done | bytes 1572880 | tf_op jit(solution)/shard_map/all_gather | solution.py:122
  231.0 2.8 convolution_bitcast_fusion.4
  233.8 23.9 %all-gather.8.cloned.1.call-done = bf16[768,1024]{1,0:T(8,128)(2,1)} async-done(((bf16[96,1024]{1,0:T(8,128)(2,1)}), bf16[768,1024]{1,0:T(8,128)(2,1)}) %all-gather.8.cloned.1.call-update) | async-done | bytes 1572880 | tf_op jit(solution)/shard_map/all_gather | solution.py:123
  257.6 1.6 convolution_bitcast_fusion.3
  259.4 4.9 %pad_maximum_fusion.1 = f32[3,512,1024]{1,2,0:T(8,128)} fusion(f32[1,512,1024]{1,2,0:T(8,128)S(1)} %convolution_bitcast_fusion.3, f32[1,512,1024]{1,2,0:T(8,128)} %convolution_bitcast_fusion.4, f32[1,512,1024]{1,2,0:T(8,128)S(1)} %copy-done.12), kind=kLoop, calls=%fused_computation.11 | loop fusion | flops 3145728 | bytes 12582912 | tf_op jit(solution)/shard_map/stack | solution.py:174
  266.4 15.0 %all-reduce.1 = bf16[768]{0:T(1024)(128)(2,1)S(1)} all-reduce(bf16[768]{0:T(1024)(128)(2,1)S(1)} %dynamic-update-slice), channel_id=1, replica_groups=mesh['ep'=4,'tp'=8] {'tp'}, use_global_device_ids=true, to_apply=%add.1 | all-reduce | flops 768 | bytes 3072
  282.1 3.6 all-to-all-start.5
  285.7 4.8 %all-to-all-done.5 = bf16[4,1,144]{2,1,0:T(2,128)(2,1)S(1)} async-done(((bf16[4,1,144]{2,1,0:T(2,128)(2,1)}), bf16[4,1,144]{2,1,0:T(2,128)(2,1)S(1)}, u32[]{:S(2)}, u32[]{:S(2)}) %all-to-all-start.5) | async-done | bytes 1184 | tf_op jit(solution)/shard_map/all_to_all | solution.py:141
  290.7 2.8 gather_fusion.3
  294.3 1.5 slice.60
  300.4 4.4 %all-to-all-start.4 = ((bf16[4,144,512]{2,1,0:T(8,128)(2,1)}), bf16[4,144,512]{2,1,0:T(8,128)(2,1)}, u32[]{:S(2)}, u32[]{:S(2)}) async-start(bf16[4,144,512]{2,1,0:T(8,128)(2,1)} %bitcast.25), calls=%async_computation.4 | async-start | bytes 1179648 | tf_op jit(solution)/shard_map/all_to_all | solution.py:134
  304.8 1.3 copy-done.8
  306.0 2.5 convolution_bitcast_fusion.1
  308.6 1.3 convolution_bitcast_fusion.2
  310.1 1.3 convolution_bitcast_fusion
  311.9 1.8 multiply_reduce_fusion
  314.0 2.3 fusion.50
  316.2 7.3 %fusion = bf16[3,2,512,1024]{3,2,1,0:T(8,128)(2,1)} fusion(f32[1,2,512,1024]{3,2,1,0:T(8,128)} %copy-done.4, f32[1,2,512,1024]{3,2,1,0:T(8,128)S(1)} %convolution_bitcast_fusion.1, f32[1,2,512,1024]{3,2,1,0:T(8,128)} %copy-done.3), kind=kLoop, calls=%fused_computation.10 | loop fusion | flops 6291456 | bytes 18874368 | tf_op jit(solution)/shard_map/convert_element_type | solution.py:189
  323.5 3.8 %gather_fusion.2 = bf16[384,512]{1,0:T(8,128)(2,1)} fusion(bf16[576,512]{1,0:T(8,128)(2,1)} %bitcast.26, s32[1024]{0:T(1024)S(1)} %pad_clamp_fusion), kind=kCustom, calls=%fused_computation.2 | custom fusion | bytes 787968 | tf_op jit(solution)/shard_map/gather | solution.py:150
  327.4 2.4 reshape.153
  329.7 2.8 reduce_sum.59
  332.6 2.4 fusion.41
  335.0 4.1 %reduce-scatter.2.cloned.1.call-done = f32[3,512,256]{1,2,0:T(8,128)} async-done(((f32[3,512,1024]{1,2,0:T(8,128)}), f32[3,512,256]{1,2,0:T(8,128)}) %reduce-scatter.2.cloned.1.call-update) | async-done | bytes 1572880 | tf_op jit(solution)/shard_map/reduce_scatter | solution.py:181
  339.1 1.6 multiply_reduce_fusion.1
  340.7 28.4 %all-reduce.2 = (f32[3,2,1024]{2,1,0:T(2,128)S(1)}, f32[3,256]{1,0:T(4,128)S(1)}) all-reduce(f32[3,2,1024]{2,1,0:T(2,128)S(1)} %multiply_reduce_fusion, f32[3,256]{1,0:T(4,128)S(1)} %multiply_reduce_fusion.1), channel_id=1, replica_groups=mesh['ep'=4,'tp'=8] {'tp'}, use_global_device_ids=true, to_apply=%region_11.12 | all-reduce | flops 6912 | bytes 55296 | tf_op jit(solution)/shard_map/psum | solution.py:184
  370.3 3.0 copy.54
  (104 shorter events, 20.7 us)
Async XLA Ops:
  7.2 52.7 %copy-start = (bf16[2,512,1024]{2,1,0:T(8,128)(2,1)S(1)}, bf16[2,512,1024]{2,1,0:T(8,128)(2,1)}, u32[]{:S(2)}) copy-start(bf16[2,512,1024]{2,1,0:T(8,128)(2,1)} %param.14) | copy-start | bytes 6291460
  7.2 9.5 %copy-start.2 = (bf16[192,512]{1,0:T(8,128)(2,1)S(1)}, bf16[192,512]{1,0:T(8,128)(2,1)}, u32[]{:S(2)}) copy-start(bf16[192,512]{1,0:T(8,128)(2,1)} %param.11) | copy-start | bytes 589828
  16.7 2.8 copy-start.1
  25.0 13.9 %all-to-all-start.2 = ((bf16[4,144,512]{2,1,0:T(8,128)(2,1)}), bf16[4,144,512]{2,1,0:T(8,128)(2,1)S(1)}, u32[]{:S(2)}, u32[]{:S(2)}) async-start(bf16[4,144,512]{2,1,0:T(8,128)(2,1)} %get-tuple-element.31), calls=%async_computation.2 | async-start | bytes 1179648 | tf_op jit(solution)/shard_map/all_to_all | solution.py:70
  32.5 13.0 %copy-start.21 = (bf16[192,2]{0,1:T(2,128)(2,1)S(1)}, bf16[192,2]{0,1:T(2,128)(2,1)}, u32[]{:S(2)}) copy-start(bf16[192,2]{0,1:T(2,128)(2,1)} %param.13) | copy-start | bytes 2308
  38.9 0.8 copy-start.13
  39.7 13.5 %all-to-all-start.1 = ((bf16[4,144,512]{2,1,0:T(8,128)(2,1)}), bf16[4,144,512]{2,1,0:T(8,128)(2,1)S(1)}, u32[]{:S(2)}, u32[]{:S(2)}) async-start(bf16[4,144,512]{2,1,0:T(8,128)(2,1)} %get-tuple-element.30), calls=%async_computation.1 | async-start | bytes 1179648 | tf_op jit(solution)/shard_map/all_to_all | solution.py:69
  53.2 6.7 %copy-start.5 = (bf16[4,144,512]{2,1,0:T(8,128)(2,1)}, bf16[4,144,512]{2,1,0:T(8,128)(2,1)S(1)}, u32[]{:S(2)}) copy-start(bf16[4,144,512]{2,1,0:T(8,128)(2,1)S(1)} %all-to-all-done.1) | copy-start | bytes 1769476
  53.2 11.6 %all-to-all-start = ((bf16[4,1,144]{2,1,0:T(2,128)(2,1)}), bf16[4,1,144]{2,1,0:T(2,128)(2,1)S(1)}, u32[]{:S(2)}, u32[]{:S(2)}) async-start(bf16[4,1,144]{2,1,0:T(2,128)(2,1)} %all_to_all.32), calls=%async_computation | async-start | bytes 8192 | tf_op jit(solution)/shard_map/all_to_all | solution.py:71
  60.6 1.3 copy-start.15
  60.7 1.3 copy-start.19
  60.8 1.4 copy-start.20
  64.8 110.2 %all-to-all-start.3 = ((bf16[8,96,3072]{2,1,0:T(8,128)(2,1)}), bf16[8,96,3072]{2,1,0:T(8,128)(2,1)}, u32[]{:S(2)}, u32[]{:S(2)}) async-start(bf16[8,96,3072]{2,1,0:T(8,128)(2,1)} %pad_maximum_fusion.2), calls=%async_computation.3 | async-start | bytes 9437184 | tf_op jit(solution)/shard_map/all_to_all | solution.py:114
  69.6 134.7 %all-gather.4.cloned.1.call-start = ((), (), s32[]{:S(2)}) async-start(), calls=%async_computation.7 | async-start | bytes 1769472 | tf_op jit(solution)/shard_map/all_gather | solution.py:121
  179.5 51.5 %all-gather.6.cloned.1.call-start = ((), (), s32[]{:S(2)}) async-start(), calls=%async_computation.8 | async-start | bytes 1769472 | tf_op jit(solution)/shard_map/all_gather | solution.py:122
  180.3 77.4 %all-gather.8.cloned.1.call-start = ((), (), s32[]{:S(2)}) async-start(), calls=%async_computation.9 | async-start | bytes 1769472 | tf_op jit(solution)/shard_map/all_gather | solution.py:123
  181.0 158.1 %reduce-scatter.2.cloned.1.call-start = ((), (), s32[]{:S(2)}) async-start(), calls=%async_computation.10 | async-start | bytes 7864320 | tf_op jit(solution)/shard_map/reduce_scatter | solution.py:181
  257.6 1.7 copy-start.12
  264.3 0.7 copy-start.22
  282.1 8.5 %all-to-all-start.5 = ((bf16[4,1,144]{2,1,0:T(2,128)(2,1)}), bf16[4,1,144]{2,1,0:T(2,128)(2,1)S(1)}, u32[]{:S(2)}, u32[]{:S(2)}) async-start(bf16[4,1,144]{2,1,0:T(2,128)(2,1)} %all_to_all.33), calls=%async_computation.5 | async-start | bytes 8192 | tf_op jit(solution)/shard_map/all_to_all | solution.py:141
  294.3 1.9 copy-start.18
  296.2 1.0 copy-start.9
  296.3 1.3 copy-start.7
  296.3 2.4 copy-start.11
  300.4 23.2 %all-to-all-start.4 = ((bf16[4,144,512]{2,1,0:T(8,128)(2,1)}), bf16[4,144,512]{2,1,0:T(8,128)(2,1)}, u32[]{:S(2)}, u32[]{:S(2)}) async-start(bf16[4,144,512]{2,1,0:T(8,128)(2,1)} %bitcast.25), calls=%async_computation.4 | async-start | bytes 1179648 | tf_op jit(solution)/shard_map/all_to_all | solution.py:134
  304.7 1.3 copy-start.8
  306.0 2.5 copy-start.6
  306.0 2.5 copy-start.10
  308.5 1.3 copy-start.14
  308.6 1.5 slice-start
  309.9 2.0 copy-start.3
  311.9 2.1 copy-start.4
  311.9 2.1 copy-start.16
  323.5 9.0 %copy-start.17 = (bf16[512,1024]{1,0:T(8,128)(2,1)S(1)}, bf16[512,1024]{1,0:T(8,128)(2,1)}, u32[]{:S(2)}) copy-start(bf16[512,1024]{1,0:T(8,128)(2,1)} %param.18) | copy-start | bytes 3145732
Sparse Core Ops, SparseCore 0:
  179.6 24.6 all-gather.3
  206.6 24.3 all-gather.5
  233.2 24.3 all-gather.7
  264.5 74.5 reduce-scatter.1
where the time goes:
time: 381 us; the launch traced here: 380 us
  waiting for transfers between devices  191 us (50%)
  blocking collectives  43.3 us (11%)
  local copies, waits for them, and re-layouts  42.8 us (11%)
  other arithmetic  31.2 us (8%)
  matrix products  30.6 us (8%)
  starting transfers between devices  25.9 us (7%)
  between operations  14.9 us (4%)
    all_to_all x1, waiting for transfers between devices, body(): lax.all_to_all(partials.reshape(tp_lanes, piece, 3 * hidden), 'tp', split...  105 us
    psum x1, blocking collectives, body(): expert_norms, shared_norms = lax.psum((expert_sq, shared_sq), 'tp')  28.4 us
    all_gather x1, waiting for transfers between devices, body(): lax.all_gather(part_scaled, 'tp', axis=0, tiled=True)  23.9 us
    all_gather x1, waiting for transfers between devices, body(): lax.all_gather(part_up, 'tp', axis=0, tiled=True)  23.8 us
    all_gather x1, waiting for transfers between devices, body(): lax.all_gather(part_gate, 'tp', axis=0, tiled=True)  23.3 us
    unnamed x1, blocking collectives  15 us
    unnamed x53, local copies, waits for them, and re-layouts  12.1 us
  transfers between devices with their start and end apart: 10, of which 7 were waited for; matrix products, arithmetic and copies ran while one was open for 16% of the time, Pallas kernels for 0%

commit v1 on v0

v1 whole, which is shorter than its diff:
```python
import functools

import jax
import jax.numpy as jnp
from jax import lax
from jax.experimental import pallas as pl
from jax.experimental.pallas import tpu as pltpu
from jax.sharding import PartitionSpec as P

MESH = pl.DeviceIdType.MESH
VMEM = pl.BlockSpec(memory_space=pltpu.VMEM)
ROWS = 16
LAG = 2
F32 = jnp.float32
BF16 = jnp.bfloat16


def enter(axis, peers):
    barrier = pltpu.get_barrier_semaphore()
    for peer in peers:
        pl.semaphore_signal(barrier, inc=1, device_id={axis: peer}, device_id_type=MESH)
    return barrier


def gather_kernel(n, tok, cot, meta, tok_out, cot_out, meta_out, send, recv, own):
    me = lax.axis_index("ep")
    peers = [lax.rem(me + s, n) for s in range(1, n)]
    barrier = enter("ep", peers)
    pl.semaphore_wait(barrier, n - 1)
    pairs = ((meta, meta_out), (tok, tok_out), (cot, cot_out))
    copies = []
    for k, (src, dst) in enumerate(pairs):
        for s, peer in enumerate(peers):
            copies.append(
                pltpu.make_async_remote_copy(
                    src_ref=src,
                    dst_ref=dst.at[me],
                    send_sem=send.at[k, s],
                    recv_sem=recv.at[k, s],
                    device_id={"ep": peer},
                    device_id_type=MESH,
                )
            )
    for copy in copies:
        copy.start()
    local = [pltpu.make_async_copy(src, dst.at[me], own.at[k]) for k, (src, dst) in enumerate(pairs)]
    for copy in local:
        copy.start()
    for copy in local:
        copy.wait()
    for copy in copies:
        copy.wait()


def gather_over_ep(tok, cot, meta):
    n = lax.axis_size("ep")
    return pl.pallas_call(
        functools.partial(gather_kernel, n),
        out_shape=[jax.ShapeDtypeStruct((n,) + a.shape, a.dtype) for a in (tok, cot, meta)],
        in_specs=[VMEM] * 3,
        out_specs=[VMEM] * 3,
        scratch_shapes=[
            pltpu.SemaphoreType.DMA((3, n - 1)),
            pltpu.SemaphoreType.DMA((3, n - 1)),
            pltpu.SemaphoreType.DMA((3,)),
        ],
        compiler_params=pltpu.CompilerParams(collective_id=0, has_side_effects=True),
        name="gather_over_ep",
    )(tok, cot, meta)


def line_kernel(n, p, w, g, wg, x, r, t, xs, xr, rs, rr, bs, br, ds, dr, vs, vr, us, ur):
    nz = n // 2
    chunks = p.shape[0] // 4
    hidden = p.shape[2] // 3
    me = lax.axis_index("tp")
    z = me // 2
    c = lax.rem(me, 2)
    partner = z * 2 + 1 - c
    right = lax.rem(z + 1, nz) * 2 + c
    left = lax.rem(z + nz - 1, nz) * 2 + c
    pos = (z, nz - 1 - z)
    onward = (right, left)
    back = (left, right)

    barrier = enter("tp", (partner, right, left))
    pl.semaphore_wait(barrier, 3)

    def remote(src, dst, ss, rsem, peer):
        return pltpu.make_async_remote_copy(
            src_ref=src, dst_ref=dst, send_sem=ss, recv_sem=rsem, device_id={"tp": peer}, device_id_type=MESH
        )

    def swap(d, j):
        return remote(p.at[(d * 2 + 1 - c) * chunks + j], x.at[d * chunks + j], xs.at[d, j], xr.at[d, j], partner)

    def hop(d, j):
        k = d * chunks + j
        return remote(t.at[k], r.at[k], rs.at[d, j], rr.at[d, j], onward[d])

    def own(d, j):
        return (d * 2 + c) * chunks + j

    def spread(d, j):
        k = own(d, j)
        return (
            remote(g.at[k], g.at[k], bs.at[d, j], br.at[d, j], back[d]),
            remote(wg.at[k], wg.at[k], vs.at[d, j], vr.at[d, j], back[d]),
        )

    def share(d, j):
        k = own(d, j)
        return (
            remote(g.at[k], g.at[k], ds.at[d, j], dr.at[d, j], partner),
            remote(wg.at[k], wg.at[k], us.at[d, j], ur.at[d, j], partner),
        )

    def first(j, _):
        for d in range(2):
            swap(d, j).start()
        return 0

    lax.fori_loop(0, chunks, first, 0)

    def step(i, _):
        for d in range(2):
            j = i - LAG * pos[d]
            live = (j >= 0) & (j < chunks)
            k = d * chunks + j
            o = own(d, j)

            @pl.when(live & (pos[d] == 0))
            def _():
                swap(d, j).wait_recv()
                t[k] = (p[o].astype(F32) + x[k].astype(F32)).astype(BF16)

            @pl.when(live & (pos[d] > 0))
            def _():
                swap(d, j).wait_recv()
                hop(d, j).wait_recv()

            @pl.when(live & (pos[d] > 0) & (pos[d] < nz - 1))
            def _():
                t[k] = (p[o].astype(F32) + x[k].astype(F32) + r[k].astype(F32)).astype(BF16)

            @pl.when(live & (pos[d] == nz - 1))
            def _():
                def total(part):
                    cols = pl.ds(part * hidden, hidden)
                    return p[o, :, cols].astype(F32) + x[k, :, cols].astype(F32) + r[k, :, cols].astype(F32)

                gate = total(0)
                up = total(1)
                bk = total(2)
                weight = w[o][:, :1]
                sig = jax.nn.sigmoid(gate)
                silu = gate * sig
                act = silu * up
                act_grad = weight * bk
                g[o, :, 0:hidden] = (act_grad * up * sig * (1.0 + gate * (1.0 - sig))).astype(BF16)
                g[o, :, hidden : 2 * hidden] = (act_grad * silu).astype(BF16)
                g[o, :, 2 * hidden : 3 * hidden] = (weight * act).astype(BF16)
                wg[o] = jnp.broadcast_to(
                    jnp.sum(act * bk, axis=1, keepdims=True), wg.shape[1:]
                ).astype(BF16)

        for d in range(2):
            j = i - LAG * pos[d]
            live = (j >= 0) & (j < chunks)

            @pl.when(live & (pos[d] < nz - 1))
            def _():
                hop(d, j).start()

            @pl.when(live & (pos[d] == nz - 1))
            def _():
                for copy in spread(d, j) + share(d, j):
                    copy.start()

        for d in range(2):
            j = i - LAG * (2 * (nz - 1) - pos[d])
            live = (j >= 0) & (j < chunks) & (pos[d] < nz - 1)

            @pl.when(live)
            def _():
                for copy in spread(d, j):
                    copy.wait_recv()

            @pl.when(live & (pos[d] > 0))
            def _():
                for copy in spread(d, j):
                    copy.start()

            @pl.when(live)
            def _():
                for copy in share(d, j):
                    copy.start()

        return 0

    lax.fori_loop(0, chunks + LAG * 2 * (nz - 1), step, 0)

    def last(j, _):
        for d in range(2):
            swap(d, j).wait_send()
            for copy in share(d, j):
                copy.wait()

            @pl.when(pos[d] < nz - 1)
            def _():
                hop(d, j).wait_send()

            @pl.when(pos[d] > 0)
            def _():
                for copy in spread(d, j):
                    copy.wait_send()

        return 0

    lax.fori_loop(0, chunks, last, 0)


def line_over_tp(p, w):
    n = lax.axis_size("tp")
    chunks = p.shape[0] // 4
    half = (2 * chunks,) + p.shape[1:]
    return pl.pallas_call(
        functools.partial(line_kernel, n),
        out_shape=[
            jax.ShapeDtypeStruct(p.shape, BF16),
            jax.ShapeDtypeStruct(p.shape[:2] + (128,), BF16),
        ],
        in_specs=[VMEM] * 2,
        out_specs=[VMEM] * 2,
        scratch_shapes=[pltpu.VMEM(half, BF16)] * 3 + [pltpu.SemaphoreType.DMA((2, chunks))] * 12,
        compiler_params=pltpu.CompilerParams(
            collective_id=1, has_side_effects=True, vmem_limit_bytes=48 * 2**20
        ),
        name="line_over_tp",
    )(p, w)


def return_kernel(ne, nt, con, gate, sq, tok_out, gate_out, sq_out, rcon, rgate, rsq, cs, cr, gs, gr, qs, qr):
    me = lax.axis_index("ep")
    mt = lax.axis_index("tp")
    ep_peers = [lax.rem(me + s, ne) for s in range(1, ne)]
    tp_peers = [lax.rem(mt + s, nt) for s in range(1, nt)]
    barrier = enter("ep", ep_peers)
    enter("tp", tp_peers)
    pl.semaphore_wait(barrier, ne + nt - 2)

    def remote(src, dst, ss, rsem, axis, peer):
        return pltpu.make_async_remote_copy(
            src_ref=src, dst_ref=dst, send_sem=ss, recv_sem=rsem, device_id={axis: peer}, device_id_type=MESH
        )

    copies = []
    for s, peer in enumerate(ep_peers):
        copies.append(remote(con.at[peer], rcon.at[s], cs.at[s], cr.at[s], "ep", peer))
    for s, peer in enumerate(tp_peers):
        copies.append(remote(sq, rsq.at[s], qs.at[s], qr.at[s], "tp", peer))
    for s, peer in enumerate(ep_peers):
        copies.append(remote(gate.at[peer], rgate.at[s], gs.at[s], gr.at[s], "ep", peer))
    for copy in copies:
        copy.start()
    for copy in copies:
        copy.wait()
    tok_out[...] = (con[me].astype(F32) + sum(rcon[s].astype(F32) for s in range(ne - 1))).astype(BF16)
    gate_out[...] = gate[me] + sum(rgate[s] for s in range(ne - 1))
    sq_out[...] = sq[...] + sum(rsq[s] for s in range(nt - 1))


def return_and_norms(con, gate, sq):
    ne, nt = lax.axis_size("ep"), lax.axis_size("tp")
    return pl.pallas_call(
        functools.partial(return_kernel, ne, nt),
        out_shape=[
            jax.ShapeDtypeStruct(con.shape[1:], BF16),
            jax.ShapeDtypeStruct(gate.shape[1:], F32),
            jax.ShapeDtypeStruct(sq.shape, F32),
        ],
        in_specs=[VMEM] * 3,
        out_specs=[VMEM] * 3,
        scratch_shapes=[
            pltpu.VMEM((ne - 1,) + con.shape[1:], BF16),
            pltpu.VMEM((ne - 1,) + gate.shape[1:], F32),
            pltpu.VMEM((nt - 1,) + sq.shape, F32),
        ]
        + [pltpu.SemaphoreType.DMA((ne - 1,))] * 4
        + [pltpu.SemaphoreType.DMA((nt - 1,))] * 2,
        compiler_params=pltpu.CompilerParams(collective_id=2, has_side_effects=True),
        name="return_and_norms",
    )(con, gate, sq)


def mm(a, b, dims):
    return lax.dot_general(a, b, (dims, ((), ())), preferred_element_type=F32)


def body(
    tokens,
    cotangent,
    routes,
    gate_weights,
    expert_gate,
    expert_up,
    expert_down,
    shared_gate,
    shared_up,
    shared_down,
):
    groups = lax.axis_size("ep")
    lanes = lax.axis_size("tp")
    here, width = tokens.shape
    choose = routes.shape[1]
    local = expert_gate.shape[0]
    hidden = expert_gate.shape[2]
    cap = 3 * here * choose // (2 * local * groups)
    slots = local * groups * cap
    part = hidden // groups
    mine = lax.axis_index("ep")

    meta = jnp.concatenate([routes.T.astype(F32), gate_weights.T.astype(F32)], axis=0)
    tok, cot, meta = gather_over_ep(tokens, cotangent, meta)
    names = meta[:, :choose].astype(jnp.int32)
    gains = meta[:, choose:]
    ids = mine * local + jnp.arange(local, dtype=jnp.int32)
    match = (names[:, None] == ids[None, :, None, None]).astype(F32)
    hit = jnp.sum(match, axis=2)
    gain = jnp.sum(match * gains[:, None], axis=2)
    before = (jnp.arange(here)[:, None] < jnp.arange(here)[None, :]).astype(BF16)
    place = mm(hit.astype(BF16).reshape(groups * local, here), before, ((1,), (0,)))
    place = place.reshape(groups, local, here)
    pick = (
        (place[:, :, None, :] == jnp.arange(cap, dtype=F32)[None, None, :, None]) & (hit[:, :, None, :] > 0)
    ).astype(BF16)
    slot_gain = jnp.sum(pick.astype(F32) * gain[:, :, None, :], axis=3)

    def take(rows, l):
        return jnp.einsum("gct,gtd->gcd", pick[:, l], rows, preferred_element_type=F32).astype(BF16).reshape(
            groups * cap, width
        )

    xs = [take(tok, l) for l in range(local)]
    gs = [take(cot, l) for l in range(local)]

    def columns(weight):
        return lax.dynamic_slice_in_dim(weight, mine * part, part, axis=1)

    sg, su, sd = columns(shared_gate), columns(shared_up), columns(shared_down)

    def side(rows, weight):
        whole = mm(rows.reshape(groups * here, width), weight, ((1,), (0,))).astype(BF16)
        return whole.reshape(groups, here, part).transpose(1, 0, 2).reshape(here, hidden)

    partials = jnp.concatenate(
        [
            jnp.concatenate(
                [
                    mm(xs[l], expert_gate[l], ((1,), (0,))).astype(BF16),
                    mm(xs[l], expert_up[l], ((1,), (0,))).astype(BF16),
                    mm(gs[l], expert_down[l], ((1,), (0,))).astype(BF16),
                ],
                axis=1,
            )
            for l in range(local)
        ]
        + [jnp.concatenate([side(tok, sg), side(tok, su), side(cot, sd)], axis=1)],
        axis=0,
    )
    weights = jnp.concatenate([slot_gain.transpose(1, 0, 2).reshape(slots), jnp.ones((here,), F32)])
    total = slots + here
    weights = jnp.broadcast_to(weights[:, None], (total, 128))
    grads, gate_sum = line_over_tp(
        partials.reshape(total // ROWS, ROWS, 3 * hidden), weights.reshape(total // ROWS, ROWS, 128)
    )
    grads = grads.reshape(total, 3 * hidden)
    gate_sum = gate_sum.reshape(total, 128)[:slots, 0].astype(F32).reshape(local, groups, cap)

    def piece(l, k):
        return grads[l * groups * cap : (l + 1) * groups * cap, k * hidden : (k + 1) * hidden]

    def tall(k):
        block = grads[slots:, k * hidden : (k + 1) * hidden]
        return block.reshape(here, groups, part).transpose(1, 0, 2).reshape(groups * here, part)

    tg, tu, ts = tall(0), tall(1), tall(2)
    con = (mm(tg, sg, ((1,), (1,))) + mm(tu, su, ((1,), (1,)))).reshape(groups, here, width)
    for l in range(local):
        slot_grad = (
            mm(piece(l, 0), expert_gate[l], ((1,), (1,))) + mm(piece(l, 1), expert_up[l], ((1,), (1,)))
        ).astype(BF16)
        con = con + jnp.einsum(
            "gct,gcd->gtd", pick[:, l], slot_grad.reshape(groups, cap, width), preferred_element_type=F32
        )
    con = con.astype(BF16)
    gate_tok = jnp.einsum("glct,lgc->glt", pick.astype(F32), gate_sum, precision=lax.Precision.HIGHEST)
    gate_con = jnp.sum(match * gate_tok[:, :, None], axis=1)

    routed = [
        jnp.stack([mm(xs[l] if k < 2 else gs[l], piece(l, k), ((0,), (0,))) for l in range(local)])
        for k in range(3)
    ]
    flat_tok, flat_cot = tok.reshape(groups * here, width), cot.reshape(groups * here, width)
    shared = [
        mm(flat_tok, tg, ((0,), (0,))),
        mm(flat_tok, tu, ((0,), (0,))),
        mm(flat_cot, ts, ((0,), (0,))),
    ]
    squares = jnp.concatenate(
        [jnp.sum(a * a, axis=1).reshape(-1) for a in routed] + [jnp.sum(a * a, axis=0) for a in shared]
    )
    count = squares.shape[0]
    pad = -count % 1024
    squares = jnp.pad(squares, (0, pad)).reshape(-1, 128)
    token_grad, gate_out, squares = return_and_norms(con, gate_con, squares)
    squares = squares.reshape(-1)[:count] * (1.0 / (width * lanes))
    routed_count = 3 * local * hidden
    return (
        token_grad,
        gate_out.T.astype(BF16),
        jnp.stack(routed).astype(BF16),
        jnp.stack(shared),
        squares[:routed_count].reshape(3, local, hidden),
        squares[routed_count:].reshape(3, part),
    )


def solution(mesh):
    return jax.shard_map(
        body,
        mesh=mesh,
        in_specs=(
            P("ep", "tp"),
            P("ep", "tp"),
            P("ep", None),
            P("ep", None),
            P("ep", "tp", None),
            P("ep", "tp", None),
            P("ep", "tp", None),
            P("tp", None),
            P("tp", None),
            P("tp", None),
        ),
        out_specs=(
            P("ep", "tp"),
            P("ep", None),
            P(None, "ep", "tp", None),
            P(None, "tp", "ep"),
            P(None, "ep", None),
            P(None, "ep"),
        ),
        check_vma=False,
    )
```

time: 381 us -> 215 us (0.56)
  waiting for transfers between devices: 191 us -> 0 us
  Pallas kernels: 0 us -> 118 us
  blocking collectives: 43.3 us -> 0 us
  local copies, waits for them, and re-layouts: 42.8 us -> 9.98 us
  other arithmetic: 31.2 us -> 59.3 us
  starting transfers between devices: 25.9 us -> 0 us
  between operations: 14.9 us -> 1.14 us
  matrix products: 30.6 us -> 25 us
    pallas_call x0 -> x3, Pallas kernels: none -> 118 us  [the longest x1 76.3 us: line_over_tp(): pl.pallas_call(functools.partial(line_kernel, n), out_shape=[jax.ShapeDty...]
    all_to_all x6 -> x0, waiting for transfers between devices: 115 us -> none  [the longest x1 105 us: body(): lax.all_to_all(partials.reshape(tp_lanes, piece, 3 * hidden), 'tp', split...]
    all_gather x3 -> x0, waiting for transfers between devices: 71 us -> none  [the longest x1 23.9 us: body(): lax.all_gather(part_scaled, 'tp', axis=0, tiled=True)]
    concatenate x5 -> x2, other arithmetic: 2.73 us -> 47.8 us  [the longest x1 47.2 us: body(): jnp.concatenate([jnp.concatenate([mm(xs[l], expert_gate[l], ((1,), (0,)))...]
    psum x1 -> x0, blocking collectives: 28.4 us -> none  [body(): expert_norms, shared_norms = lax.psum((expert_sq, shared_sq), 'tp')]
    all_to_all x6 -> x0, starting transfers between devices: 25.7 us -> none  [the longest x1 5.19 us: body(): lax.all_to_all(send_cotan, 'ep', split_axis=0, concat_axis=0, tiled=True)]
    unnamed x1 -> x0, blocking collectives: 15 us -> none
    gather x4 -> x0, local copies, waits for them, and re-layouts: 12.6 us -> none  [the longest x1 3.82 us: body(): back_rows.reshape(total_slots, feat_width)[slot_index].astype(jnp.float32)]
  transfers between devices with their start and end apart: 10 -> 0, of which waited for: 7 -> 0; matrix products, arithmetic and copies ran while one was open for 16% -> 0% of each run, Pallas kernels for 0% -> 0%
where the time goes in v1:
time: 215 us; the launch traced here: 214 us
  Pallas kernels  118 us (55%)
  other arithmetic  59.3 us (28%)
  matrix products  25 us (12%)
  local copies, waits for them, and re-layouts  9.98 us (5%)
    pallas_call x1, Pallas kernels, line_over_tp(): pl.pallas_call(functools.partial(line_kernel, n), out_shape=[jax.ShapeDty...  76.3 us
    concatenate x1, other arithmetic, body(): jnp.concatenate([jnp.concatenate([mm(xs[l], expert_gate[l], ((1,), (0,)))...  47.2 us
    pallas_call x1, Pallas kernels, gather_over_ep(): pl.pallas_call(functools.partial(gather_kernel, n), out_shape=[jax.ShapeD...  24.3 us
    dot_general x25, matrix products, mm(): return lax.dot_general(a, b, (dims, ((), ())), preferred_element_type=F32)  19.7 us
    pallas_call x1, Pallas kernels, return_and_norms(): pl.pallas_call(functools.partial(return_kernel, ne, nt), out_shape=[jax.S...  17.8 us
    unnamed x37, local copies, waits for them, and re-layouts  5.88 us

profile of v1, /device:TPU:0, one launch (start us, length us, event | category | flops | bytes accessed | tf_op | source)
XLA Modules:
  0.0 213.9 jit_solution(13385887665102740762)
XLA Ops:
  0.7 0.8 convert_bitcast_fusion.1
  1.4 0.7 convert_bitcast_fusion
  2.1 0.6 pad_maximum_fusion.5.meta
  2.7 24.3 %gather_over_ep.1 = (bf16[4,192,512]{2,1,0:T(8,128)(2,1)}, bf16[4,192,512]{2,1,0:T(8,128)(2,1)}, f32[4,4,192]{2,1,0:T(4,128)}) custom-call(bf16[192,512]{1,0:T(8,128)(2,1)} %tok.1, bf16[192,512]{1,0:T(8,128)(2,1)} %cot.1, f32[4,192]{1,0:T(4,128)} %pad_maximum_fusion.5.meta), custom_call_target="tpu_custom_call" | custom-call | tf_op jit(solution)/shard_map/gather_over_ep/pallas_call | solution.py:57
  27.1 0.8 slice_convert_fusion
  28.7 1.4 convolution_convert_fusion.11
  30.1 1.5 convolution_convert_fusion.9
  32.4 1.3 convolution_convert_fusion.6
  34.1 1.3 convolution_convert_fusion.7
  36.6 0.7 copy-done.12
  37.3 0.5 convolution_convert_fusion.4
  38.0 0.5 convolution_convert_fusion.5
  38.5 0.5 convolution_convert_fusion.1
  39.0 0.5 convolution_convert_fusion.2
  39.5 0.6 copy-done.10
  40.1 0.5 convolution_convert_fusion
  40.6 0.5 convolution_convert_fusion.3
  41.1 47.2 %maximum_maximum_fusion = bf16[768,3072]{1,0:T(8,128)(2,1)} fusion(bf16[192,1024]{1,0:T(8,128)(2,1)S(1)} %bitcast.211, bf16[192,1024]{1,0:T(8,128)(2,1)S(1)} %bitcast.212, bf16[192,1024]{1,0:T(8,128)(2,1)S(1)} %bitcast.213, bf16[288,1024]{1,0:T(8,128)(2,1)S(1)} %convolution_convert_fusion, bf16[288,1024]{1,0:T(8,128)(2,1)S(1)} %convolution_convert_fusion.1, ...), kind=kLoop, calls=%fused_computation.1 | loop fusion | flops 42467328 | bytes 9437184 | tf_op jit(solution)/shard_map/concatenate | solution.py:356
  88.3 76.3 %line_over_tp.1 = (bf16[48,16,3072]{2,1,0:T(8,128)(2,1)S(1)}, bf16[48,16,128]{2,1,0:T(8,128)(2,1)S(1)}) custom-call(bf16[48,16,3072]{2,1,0:T(8,128)(2,1)} %bitcast.198, f32[48,16,128]{2,1,0:T(8,128)S(1)} %broadcast_in_dim.5.w), custom_call_target="tpu_custom_call" | custom-call | tf_op jit(solution)/shard_map/line_over_tp/pallas_call | solution.py:227
  164.6 2.2 %copy-done.2 = bf16[48,16,3072]{2,1,0:T(8,128)(2,1)} copy-done((bf16[48,16,3072]{2,1,0:T(8,128)(2,1)}, bf16[48,16,3072]{2,1,0:T(8,128)(2,1)S(1)}, u32[]{:S(2)}) %copy-start.2) | copy-done | bytes 4718616
  167.3 0.6 copy.45.gate
  167.9 2.1 fusion.11
  169.9 2.1 fusion.7
  172.0 1.7 fusion.17
  173.8 0.5 fusion.6
  174.4 0.4 fusion.35
  174.8 0.4 fusion.36
  175.3 0.4 fusion.37
  175.7 1.2 pad_maximum_fusion.4
  177.4 1.3 convolution_add_fusion
  179.2 1.3 add_convert_fusion.con
  180.5 0.7 convolution_bitcast_fusion
  181.4 0.7 convolution_bitcast_fusion.1
  183.0 0.7 convolution_bitcast_fusion.4
  183.7 0.7 convolution_bitcast_fusion.2
  184.4 0.7 convolution_bitcast_fusion.5
  185.2 0.7 convolution_bitcast_fusion.3
  185.9 0.4 multiply_reduce_fusion.1
  186.3 0.7 fusion.3
  187.0 0.4 multiply_reduce_fusion.2
  187.5 3.1 %pad_maximum_fusion = bf16[3,2,512,1024]{3,2,1,0:T(8,128)(2,1)} fusion(bf16[1,2,512,1024]{3,2,1,0:T(8,128)(2,1)S(1)} %fusion.5, bf16[1,2,512,1024]{3,2,1,0:T(8,128)(2,1)S(1)} %get-tuple-element.36, bf16[1,2,512,1024]{3,2,1,0:T(8,128)(2,1)S(1)} %get-tuple-element.35), kind=kLoop, calls=%fused_computation | loop fusion | flops 6291456 | bytes 12582912 | tf_op jit(solution)/shard_map/stack | solution.py:422
  190.7 0.6 pad_bitcast_fusion.sq
  191.3 17.8 %return_and_norms.1 = (bf16[192,512]{1,0:T(8,128)(2,1)}, f32[2,192]{1,0:T(2,128)}, f32[56,128]{1,0:T(8,128)}) custom-call(bf16[4,192,512]{2,1,0:T(8,128)(2,1)} %add_convert_fusion.con, f32[4,2,192]{2,1,0:T(2,128)} %copy.45.gate, f32[56,128]{1,0:T(8,128)} %pad_bitcast_fusion.sq), custom_call_target="tpu_custom_call" | custom-call | tf_op jit(solution)/shard_map/return_and_norms/pallas_call | solution.py:275
  209.1 1.2 convert_bitcast_fusion.2
  210.3 0.8 slice_multiply_fusion
  211.1 0.6 reshape.175
  211.7 0.6 slice.110
  212.3 1.6 copy.95
  (66 shorter events, 5.8 us)
Async XLA Ops:
  0.6 35.1 %copy-start = (bf16[512,1024]{1,0:T(8,128)(2,1)S(1)}, bf16[512,1024]{1,0:T(8,128)(2,1)}, u32[]{:S(2)}) copy-start(bf16[512,1024]{1,0:T(8,128)(2,1)} %param.17) | copy-start | bytes 3145732
  27.1 4.6 %copy-start.4 = (bf16[4,192,512]{2,1,0:T(8,128)(2,1)S(1)}, bf16[4,192,512]{2,1,0:T(8,128)(2,1)}, u32[]{:S(2)}) copy-start(bf16[4,192,512]{2,1,0:T(8,128)(2,1)} %get-tuple-element.15) | copy-start | bytes 2359300
  30.1 10.5 %copy-start.6 = (bf16[4,72,512]{2,1,0:T(8,128)(2,1)}, bf16[4,72,512]{2,1,0:T(8,128)(2,1)S(1)}, u32[]{:S(2)}) copy-start(bf16[4,72,512]{2,1,0:T(8,128)(2,1)S(1)} %convolution_convert_fusion.11) | copy-start | bytes 884740
  30.1 2.2 %copy-start.5 = (bf16[4,192,512]{2,1,0:T(8,128)(2,1)S(1)}, bf16[4,192,512]{2,1,0:T(8,128)(2,1)}, u32[]{:S(2)}) copy-start(bf16[4,192,512]{2,1,0:T(8,128)(2,1)} %get-tuple-element.16) | copy-start | bytes 2359300
  31.6 7.9 %copy-start.8 = (bf16[4,72,512]{2,1,0:T(8,128)(2,1)}, bf16[4,72,512]{2,1,0:T(8,128)(2,1)S(1)}, u32[]{:S(2)}) copy-start(bf16[4,72,512]{2,1,0:T(8,128)(2,1)S(1)} %convolution_convert_fusion.9) | copy-start | bytes 884740
  35.7 1.6 copy-start.12
  36.2 1.9 copy-start.11
  38.5 1.6 copy-start.10
  164.6 2.2 %copy-start.2 = (bf16[48,16,3072]{2,1,0:T(8,128)(2,1)}, bf16[48,16,3072]{2,1,0:T(8,128)(2,1)S(1)}, u32[]{:S(2)}) copy-start(bf16[48,16,3072]{2,1,0:T(8,128)(2,1)S(1)} %get-tuple-element.17) | copy-start | bytes 14155780
  167.9 4.2 %copy-start.3 = (bf16[48,16,3072]{2,1,0:T(8,128)(2,1)S(1)}, bf16[48,16,3072]{2,1,0:T(8,128)(2,1)}, u32[]{:S(2)}) copy-start(bf16[48,16,3072]{2,1,0:T(8,128)(2,1)} %copy-done.2) | copy-start | bytes 14155780
  169.9 3.8 %copy-start.13 = (bf16[2,512,1024]{2,1,0:T(8,128)(2,1)S(1)}, bf16[2,512,1024]{2,1,0:T(8,128)(2,1)}, u32[]{:S(2)}) copy-start(bf16[2,512,1024]{2,1,0:T(8,128)(2,1)} %param.15) | copy-start | bytes 6291460
  179.2 1.3 copy-start.9
  180.5 1.0 copy-start.7
  187.5 26.4 %copy-start.1 = (bf16[512,1024]{1,0:T(8,128)(2,1)S(1)}, bf16[512,1024]{1,0:T(8,128)(2,1)}, u32[]{:S(2)}) copy-start(bf16[512,1024]{1,0:T(8,128)(2,1)} %param.17) | copy-start | bytes 3145732

commit v2 on v1

--- a/solution.py
+++ b/solution.py
@@ -11,6 +11,7 @@
 VMEM = pl.BlockSpec(memory_space=pltpu.VMEM)
 ROWS = 16
 LAG = 2
+TILE = 256
 F32 = jnp.float32
 BF16 = jnp.bfloat16
 
@@ -69,10 +70,21 @@
     )(tok, cot, meta)
 
 
-def line_kernel(n, p, w, g, wg, x, r, t, xs, xr, rs, rr, bs, br, ds, dr, vs, vr, us, ur):
+def tiles(size):
+    step = min(TILE, size)
+    return size // step, step
+
+
+def line_kernel(n, local, *refs):
+    rows, refs = (refs[:local], refs[local : 2 * local]), refs[2 * local :]
+    tok, cot, eg, eu, ed, sg, su, sd, w, g, p, x, r, t, xs, xr, rs, rr, bs, br, ds, dr = refs
     nz = n // 2
     chunks = p.shape[0] // 4
     hidden = p.shape[2] // 3
+    part = sg.shape[1]
+    carry = t.dtype
+    each = rows[0][0].shape[0] // ROWS
+    tail = tok.shape[1] // ROWS
     me = lax.axis_index("tp")
     z = me // 2
     c = lax.rem(me, 2)
@@ -84,6 +96,25 @@
     back = (left, right)
 
     barrier = enter("tp", (partner, right, left))
+
+    amount, size = tiles(hidden)
+    for l in range(local):
+        for k, (block, weight) in enumerate(((rows[0][l], eg), (rows[0][l], eu), (rows[1][l], ed))):
+
+            def project(i, _, block=block, weight=weight, k=k, l=l):
+                cols = pl.ds(pl.multiple_of(i * size, size), size)
+                into = pl.ds(pl.multiple_of(k * hidden + i * size, size), size)
+                value = jnp.dot(block[...], weight[l, :, cols], preferred_element_type=F32)
+                p[l * each : (l + 1) * each, :, into] = value.astype(BF16).reshape(each, ROWS, size)
+                return 0
+
+            lax.fori_loop(0, amount, project, 0)
+    for k, (block, weight) in enumerate(((tok, sg), (tok, su), (cot, sd))):
+        for b in range(tok.shape[0]):
+            value = jnp.dot(block[b], weight[...], preferred_element_type=F32).astype(BF16)
+            start = k * hidden + b * part
+            p[local * each :, :, start : start + part] = value.reshape(tail, ROWS, part)
+
     pl.semaphore_wait(barrier, 3)
 
     def remote(src, dst, ss, rsem, peer):
@@ -103,17 +134,11 @@
 
     def spread(d, j):
         k = own(d, j)
-        return (
-            remote(g.at[k], g.at[k], bs.at[d, j], br.at[d, j], back[d]),
-            remote(wg.at[k], wg.at[k], vs.at[d, j], vr.at[d, j], back[d]),
-        )
+        return (remote(g.at[k], g.at[k], bs.at[d, j], br.at[d, j], back[d]),)
 
     def share(d, j):
         k = own(d, j)
-        return (
-            remote(g.at[k], g.at[k], ds.at[d, j], dr.at[d, j], partner),
-            remote(wg.at[k], wg.at[k], us.at[d, j], ur.at[d, j], partner),
-        )
+        return (remote(g.at[k], g.at[k], ds.at[d, j], dr.at[d, j], partner),)
 
     def first(j, _):
         for d in range(2):
@@ -132,7 +157,7 @@
             @pl.when(live & (pos[d] == 0))
             def _():
                 swap(d, j).wait_recv()
-                t[k] = (p[o].astype(F32) + x[k].astype(F32)).astype(BF16)
+                t[k] = (p[o].astype(F32) + x[k].astype(F32)).astype(carry)
 
             @pl.when(live & (pos[d] > 0))
             def _():
@@ -141,7 +166,7 @@
 
             @pl.when(live & (pos[d] > 0) & (pos[d] < nz - 1))
             def _():
-                t[k] = (p[o].astype(F32) + x[k].astype(F32) + r[k].astype(F32)).astype(BF16)
+                t[k] = (p[o].astype(F32) + x[k].astype(F32) + r[k].astype(F32)).astype(carry)
 
             @pl.when(live & (pos[d] == nz - 1))
             def _():
@@ -160,8 +185,8 @@
                 g[o, :, 0:hidden] = (act_grad * up * sig * (1.0 + gate * (1.0 - sig))).astype(BF16)
                 g[o, :, hidden : 2 * hidden] = (act_grad * silu).astype(BF16)
                 g[o, :, 2 * hidden : 3 * hidden] = (weight * act).astype(BF16)
-                wg[o] = jnp.broadcast_to(
-                    jnp.sum(act * bk, axis=1, keepdims=True), wg.shape[1:]
+                g[o, :, 3 * hidden :] = jnp.broadcast_to(
+                    jnp.sum(act * bk, axis=1, keepdims=True), (ROWS, 128)
                 ).astype(BF16)
 
         for d in range(2):
@@ -220,27 +245,37 @@
     lax.fori_loop(0, chunks, last, 0)
 
 
-def line_over_tp(p, w):
+def line_over_tp(xs, gs, tok, cot, eg, eu, ed, sg, su, sd, w):
     n = lax.axis_size("tp")
-    chunks = p.shape[0] // 4
-    half = (2 * chunks,) + p.shape[1:]
+    blocks, hidden = w.shape[0], eg.shape[2]
+    carry = BF16 if n <= 8 else F32
+    full = (blocks, ROWS, 3 * hidden)
+    half = (blocks // 2, ROWS, 3 * hidden)
+    args = (*xs, *gs, tok, cot, eg, eu, ed, sg, su, sd, w)
     return pl.pallas_call(
-        functools.partial(line_kernel, n),
-        out_shape=[
-            jax.ShapeDtypeStruct(p.shape, BF16),
-            jax.ShapeDtypeStruct(p.shape[:2] + (128,), BF16),
-        ],
-        in_specs=[VMEM] * 2,
-        out_specs=[VMEM] * 2,
-        scratch_shapes=[pltpu.VMEM(half, BF16)] * 3 + [pltpu.SemaphoreType.DMA((2, chunks))] * 12,
+        functools.partial(line_kernel, n, len(xs)),
+        out_shape=jax.ShapeDtypeStruct((blocks, ROWS, 3 * hidden + 128), BF16),
+        in_specs=[VMEM] * len(args),
+        out_specs=VMEM,
+        scratch_shapes=[
+            pltpu.VMEM(full, BF16),
+            pltpu.VMEM(half, BF16),
+            pltpu.VMEM(half, carry),
+            pltpu.VMEM(half, carry),
+        ]
+        + [pltpu.SemaphoreType.DMA((2, blocks // 4))] * 8,
         compiler_params=pltpu.CompilerParams(
             collective_id=1, has_side_effects=True, vmem_limit_bytes=48 * 2**20
         ),
         name="line_over_tp",
-    )(p, w)
-
-
-def return_kernel(ne, nt, con, gate, sq, tok_out, gate_out, sq_out, rcon, rgate, rsq, cs, cr, gs, gr, qs, qr):
+    )(*args)
+
+
+def return_kernel(ne, nt, local, *refs):
+    lhs, refs = (refs[:local], refs[local : 2 * local]), refs[2 * local :]
+    tokt, cott, tg, tu, ts, grads, con, gate = refs[:8]
+    tok_out, gate_out, sq_out, eg_out, sh_out = refs[8:13]
+    sq, rcon, rgate, rsq, cs, cr, gs, gr, qs, qr = refs[13:]
     me = lax.axis_index("ep")
     mt = lax.axis_index("tp")
     ep_peers = [lax.rem(me + s, ne) for s in range(1, ne)]
@@ -257,40 +292,76 @@
     copies = []
     for s, peer in enumerate(ep_peers):
         copies.append(remote(con.at[peer], rcon.at[s], cs.at[s], cr.at[s], "ep", peer))
-    for s, peer in enumerate(tp_peers):
-        copies.append(remote(sq, rsq.at[s], qs.at[s], qr.at[s], "tp", peer))
-    for s, peer in enumerate(ep_peers):
         copies.append(remote(gate.at[peer], rgate.at[s], gs.at[s], gr.at[s], "ep", peer))
     for copy in copies:
+        copy.start()
+
+    sq[...] = jnp.zeros_like(sq)
+    hidden = eg_out.shape[3]
+    part = sh_out.shape[2]
+    each = lhs[0][0].shape[1]
+    deep = each // ROWS
+    amount, size = tiles(hidden)
+    for k, (block, right) in enumerate(((tokt, tg), (tokt, tu), (cott, ts))):
+        value = jnp.dot(block[...], right[...], preferred_element_type=F32)
+        sh_out[k] = value
+        sq[3 * local : 3 * local + 1, k * part : (k + 1) * part] = jnp.sum(value * value, axis=0, keepdims=True)
+    for l in range(local):
+        for k in range(3):
+
+            def weigh(i, _, k=k, l=l):
+                cols = pl.ds(pl.multiple_of(i * size, size), size)
+                src = pl.ds(pl.multiple_of(k * hidden + i * size, size), size)
+                right = grads[l * deep : (l + 1) * deep, :, src].reshape(each, size)
+                value = jnp.dot(lhs[k // 2][l][...], right, preferred_element_type=F32)
+                eg_out[k, l, :, cols] = value.astype(BF16)
+                sq[k * local + l : k * local + l + 1, cols] = jnp.sum(value * value, axis=0, keepdims=True)
+                return 0
+
+            lax.fori_loop(0, amount, weigh, 0)
+
+    sums = [remote(sq, rsq.at[s], qs.at[s], qr.at[s], "tp", peer) for s, peer in enumerate(tp_peers)]
+    for copy in sums:
         copy.start()
     for copy in copies:
         copy.wait()
     tok_out[...] = (con[me].astype(F32) + sum(rcon[s].astype(F32) for s in range(ne - 1))).astype(BF16)
     gate_out[...] = gate[me] + sum(rgate[s] for s in range(ne - 1))
-    sq_out[...] = sq[...] + sum(rsq[s] for s in range(nt - 1))
-
-
-def return_and_norms(con, gate, sq):
+    for copy in sums:
+        copy.wait()
+    sq_out[...] = (sq[...] + sum(rsq[s] for s in range(nt - 1))) * (1.0 / (tokt.shape[0] * nt))
+
+
+def return_and_norms(xt, gt, tokt, cott, tg, tu, ts, grads, con, gate):
     ne, nt = lax.axis_size("ep"), lax.axis_size("tp")
+    local = len(xt)
+    width, hidden, part = tokt.shape[0], (grads.shape[2] - 128) // 3, tg.shape[1]
+    sq_shape = (-(-(3 * local + 1) // 8) * 8, hidden)
+    args = (*xt, *gt, tokt, cott, tg, tu, ts, grads, con, gate)
     return pl.pallas_call(
-        functools.partial(return_kernel, ne, nt),
+        functools.partial(return_kernel, ne, nt, local),
         out_shape=[
             jax.ShapeDtypeStruct(con.shape[1:], BF16),
             jax.ShapeDtypeStruct(gate.shape[1:], F32),
-            jax.ShapeDtypeStruct(sq.shape, F32),
+            jax.ShapeDtypeStruct(sq_shape, F32),
+            jax.ShapeDtypeStruct((3, local, width, hidden), BF16),
+            jax.ShapeDtypeStruct((3, width, part), F32),
         ],
-        in_specs=[VMEM] * 3,
-        out_specs=[VMEM] * 3,
+        in_specs=[VMEM] * len(args),
+        out_specs=[VMEM] * 5,
         scratch_shapes=[
+            pltpu.VMEM(sq_shape, F32),
             pltpu.VMEM((ne - 1,) + con.shape[1:], BF16),
             pltpu.VMEM((ne - 1,) + gate.shape[1:], F32),
-            pltpu.VMEM((nt - 1,) + sq.shape, F32),
+            pltpu.VMEM((nt - 1,) + sq_shape, F32),
         ]
         + [pltpu.SemaphoreType.DMA((ne - 1,))] * 4
         + [pltpu.SemaphoreType.DMA((nt - 1,))] * 2,
-        compiler_params=pltpu.CompilerParams(collective_id=2, has_side_effects=True),
+        compiler_params=pltpu.CompilerParams(
+            collective_id=2, has_side_effects=True, vmem_limit_bytes=40 * 2**20
+        ),
         name="return_and_norms",
-    )(con, gate, sq)
+    )(*args)
 
 
 def mm(a, b, dims):
@@ -349,33 +420,24 @@
 
     sg, su, sd = columns(shared_gate), columns(shared_up), columns(shared_down)
 
-    def side(rows, weight):
-        whole = mm(rows.reshape(groups * here, width), weight, ((1,), (0,))).astype(BF16)
-        return whole.reshape(groups, here, part).transpose(1, 0, 2).reshape(here, hidden)
-
-    partials = jnp.concatenate(
-        [
-            jnp.concatenate(
-                [
-                    mm(xs[l], expert_gate[l], ((1,), (0,))).astype(BF16),
-                    mm(xs[l], expert_up[l], ((1,), (0,))).astype(BF16),
-                    mm(gs[l], expert_down[l], ((1,), (0,))).astype(BF16),
-                ],
-                axis=1,
-            )
-            for l in range(local)
-        ]
-        + [jnp.concatenate([side(tok, sg), side(tok, su), side(cot, sd)], axis=1)],
-        axis=0,
-    )
     weights = jnp.concatenate([slot_gain.transpose(1, 0, 2).reshape(slots), jnp.ones((here,), F32)])
     total = slots + here
     weights = jnp.broadcast_to(weights[:, None], (total, 128))
-    grads, gate_sum = line_over_tp(
-        partials.reshape(total // ROWS, ROWS, 3 * hidden), weights.reshape(total // ROWS, ROWS, 128)
+    blocks = line_over_tp(
+        xs,
+        gs,
+        tok,
+        cot,
+        expert_gate,
+        expert_up,
+        expert_down,
+        sg,
+        su,
+        sd,
+        weights.reshape(total // ROWS, ROWS, 128),
     )
-    grads = grads.reshape(total, 3 * hidden)
-    gate_sum = gate_sum.reshape(total, 128)[:slots, 0].astype(F32).reshape(local, groups, cap)
+    grads = blocks.reshape(total, 3 * hidden + 128)
+    gate_sum = grads[:slots, 3 * hidden].astype(F32).reshape(local, groups, cap)
 
     def piece(l, k):
         return grads[l * groups * cap : (l + 1) * groups * cap, k * hidden : (k + 1) * hidden]
@@ -397,32 +459,25 @@
     gate_tok = jnp.einsum("glct,lgc->glt", pick.astype(F32), gate_sum, precision=lax.Precision.HIGHEST)
     gate_con = jnp.sum(match * gate_tok[:, :, None], axis=1)
 
-    routed = [
-        jnp.stack([mm(xs[l] if k < 2 else gs[l], piece(l, k), ((0,), (0,))) for l in range(local)])
-        for k in range(3)
-    ]
-    flat_tok, flat_cot = tok.reshape(groups * here, width), cot.reshape(groups * here, width)
-    shared = [
-        mm(flat_tok, tg, ((0,), (0,))),
-        mm(flat_tok, tu, ((0,), (0,))),
-        mm(flat_cot, ts, ((0,), (0,))),
-    ]
-    squares = jnp.concatenate(
-        [jnp.sum(a * a, axis=1).reshape(-1) for a in routed] + [jnp.sum(a * a, axis=0) for a in shared]
+    token_grad, gate_out, squares, routed, shared = return_and_norms(
+        [a.T for a in xs],
+        [a.T for a in gs],
+        tok.reshape(groups * here, width).T,
+        cot.reshape(groups * here, width).T,
+        tg,
+        tu,
+        ts,
+        blocks,
+        con,
+        gate_con,
     )
-    count = squares.shape[0]
-    pad = -count % 1024
-    squares = jnp.pad(squares, (0, pad)).reshape(-1, 128)
-    token_grad, gate_out, squares = return_and_norms(con, gate_con, squares)
-    squares = squares.reshape(-1)[:count] * (1.0 / (width * lanes))
-    routed_count = 3 * local * hidden
     return (
         token_grad,
         gate_out.T.astype(BF16),
-        jnp.stack(routed).astype(BF16),
-        jnp.stack(shared),
-        squares[:routed_count].reshape(3, local, hidden),
-        squares[routed_count:].reshape(3, part),
+        routed,
+        shared,
+        squares[: 3 * local].reshape(3, local, hidden),
+        squares[3 * local, : 3 * part].reshape(3, part),
     )
 
 

time: 215 us -> 195 us (0.907)
  other arithmetic: 59.3 us -> 4.78 us
  local copies, waits for them, and re-layouts: 9.98 us -> 45.3 us
  matrix products: 25 us -> 15.4 us
  Pallas kernels: 118 us -> 127 us
    concatenate x1 -> x0, other arithmetic: 47.2 us -> none  [body(): jnp.concatenate([jnp.concatenate([mm(xs[l], expert_gate[l], ((1,), (0,)))...]
    unnamed x37 -> x75, local copies, waits for them, and re-layouts: 5.88 us -> 23.7 us
    dot_general x25 -> x7, matrix products: 19.7 us -> 9.14 us  [mm(): return lax.dot_general(a, b, (dims, ((), ())), preferred_element_type=F32)]
    pallas_call x2, Pallas kernels: 94 us -> 103 us  [the longest x1 82.2 us: line_over_tp(): pl.pallas_call(functools.partial(line_kernel, n, len(xs)), out_shape=jax....]
    another operation x4 -> x0, other arithmetic: 5.47 us -> none  [the longest x3 4.23 us: body(): jnp.stack(routed).astype(BF16)]
    reshape x6 -> x8, local copies, waits for them, and re-layouts: 2.25 us -> 6.82 us  [the longest x4 4.68 us: take(): jnp.einsum('gct,gtd->gcd', pick[:, l], rows, preferred_element_type=F32)]
    reshape x2 -> x3, local copies, waits for them, and re-layouts: 0.05 us -> 4.12 us  [tall(): block.reshape(here, groups, part).transpose(1, 0, 2)]
    transpose x0 -> x3, local copies, waits for them, and re-layouts: none -> 3.19 us  [tall(): block.reshape(here, groups, part).transpose(1, 0, 2)]
where the time goes in v2:
time: 195 us; the launch traced here: 194 us
  Pallas kernels  127 us (65%)
  local copies, waits for them, and re-layouts  45.3 us (23%)
  matrix products  15.4 us (8%)
  other arithmetic  4.78 us (2%)
    pallas_call x1, Pallas kernels, line_over_tp(): pl.pallas_call(functools.partial(line_kernel, n, len(xs)), out_shape=jax....  82.2 us
    pallas_call x1, Pallas kernels, gather_over_ep(): pl.pallas_call(functools.partial(gather_kernel, n), out_shape=[jax.ShapeD...  24.4 us
    unnamed x75, local copies, waits for them, and re-layouts  23.7 us
    pallas_call x1, Pallas kernels, return_and_norms(): pl.pallas_call(functools.partial(return_kernel, ne, nt, local), out_shape...  20.5 us
    dot_general x7, matrix products, mm(): return lax.dot_general(a, b, (dims, ((), ())), preferred_element_type=F32)  9.14 us
    reshape x4, local copies, waits for them, and re-layouts, take(): jnp.einsum('gct,gtd->gcd', pick[:, l], rows, preferred_element_type=F32)  4.68 us
    dot_general x4, matrix products, take(): jnp.einsum('gct,gtd->gcd', pick[:, l], rows, preferred_element_type=F32)  4.17 us
    reshape x3, local copies, waits for them, and re-layouts, tall(): block.reshape(here, groups, part).transpose(1, 0, 2)  4.12 us

profile of v2, /device:TPU:0, one launch (start us, length us, event | category | flops | bytes accessed | tf_op | source)
XLA Modules:
  0.0 193.5 jit_solution(8905123944602978892)
XLA Ops:
  0.7 0.8 convert_bitcast_fusion.1
  1.4 0.7 convert_bitcast_fusion
  2.1 0.6 pad_maximum_fusion.meta
  2.7 0.7 constant_dynamic-slice_fusion.2.refs_9_
  3.5 1.9 constant_dynamic-slice_fusion
  5.4 24.4 %gather_over_ep.1 = (bf16[4,192,512]{2,1,0:T(8,128)(2,1)}, bf16[4,192,512]{2,1,0:T(8,128)(2,1)}, f32[4,4,192]{2,1,0:T(4,128)}) custom-call(bf16[192,512]{1,0:T(8,128)(2,1)} %tok.1, bf16[192,512]{1,0:T(8,128)(2,1)} %cot.1, f32[4,192]{1,0:T(4,128)} %pad_maximum_fusion.meta), custom_call_target="tpu_custom_call" | custom-call | tf_op jit(solution)/shard_map/gather_over_ep/pallas_call | solution.py:58
  29.7 0.8 slice_convert_fusion
  32.0 1.4 convolution_convert_fusion.1
  33.4 1.5 convolution_convert_fusion
  35.3 1.0 convolution_convert_fusion.3
  36.2 0.9 broadcast_in_dim.5.refs_12_
  37.2 1.9 copy.50
  39.0 0.9 copy.51
  40.0 0.9 copy.53
  40.9 0.9 copy.52
  42.1 1.2 copy.54
  43.3 1.0 copy-done.5
  44.2 1.0 copy-done.7
  45.2 1.0 copy-done.9
  46.2 1.0 copy-done.10
  47.1 0.9 copy-done.11
  48.1 0.9 copy-done.13
  49.0 1.6 copy-done.15
  50.6 1.0 copy-done.23
  51.6 0.9 copy-done.24
  52.6 82.2 %line_over_tp.1.refs_9_ = bf16[48,16,3200]{2,1,0:T(8,128)(2,1)} custom-call(bf16[288,512]{1,0:T(8,128)(2,1)S(1)} %bitcast.91, bf16[288,512]{1,0:T(8,128)(2,1)S(1)} %bitcast.89, bf16[288,512]{1,0:T(8,128)(2,1)S(1)} %bitcast.85, bf16[288,512]{1,0:T(8,128)(2,1)S(1)} %bitcast.87, bf16[4,192,512]{2,1,0:T(8,128)(2,1)S(1)} %copy-done.1, ...), custom_call_target="tpu_custom_call" | custom-call | tf_op jit(solution)/shard_map/line_over_tp/pallas_call | solution.py:255
  134.8 1.1 slice_reduce_fusion
  136.1 0.9 fusion.25
  137.1 1.9 fusion.3
  139.0 2.4 %fusion.1 = bf16[288,512]{1,0:T(8,128)(2,1)} fusion(f32[288,512]{1,0:T(8,128)S(1)} %fusion.3, bf16[2,512,1024]{2,1,0:T(8,128)(2,1)S(1)} %copy-done.30, bf16[768,3200]{1,0:T(8,128)(2,1)} %bitcast.70), kind=kOutput, calls=%fused_computation.5 | convolution fusion | flops 302284800 | bytes 2523136 | tf_op jit(solution)/shard_map/dot_general | solution.py:368
  141.4 1.6 fusion.6
  143.0 2.3 %fusion = bf16[288,512]{1,0:T(8,128)(2,1)} fusion(f32[288,512]{1,0:T(8,128)S(1)} %fusion.6, bf16[2,512,1024]{2,1,0:T(8,128)(2,1)S(1)} %copy-done.30, bf16[768,3200]{1,0:T(8,128)(2,1)} %bitcast.72), kind=kOutput, calls=%fused_computation.4 | convolution fusion | flops 302284800 | bytes 2523136 | tf_op jit(solution)/shard_map/dot_general | solution.py:368
  145.3 2.1 %fusion.28 = (bf16[192,1024]{1,0:T(8,128)(2,1)S(1)}, bf16[192,1024]{1,0:T(8,128)(2,1)S(1)}, bf16[192,1024]{1,0:T(8,128)(2,1)}) fusion(bf16[768,3200]{1,0:T(8,128)(2,1)} %bitcast.73), kind=kLoop, calls=%fused_computation.56 | loop fusion | bytes 2359296 | tf_op jit(solution)/shard_map/slice | solution.py:446
  147.4 1.0 reshape.109
  148.4 1.1 copy.59
  149.5 1.0 reshape.107
  150.6 1.1 copy.58
  151.6 2.0 %reshape.105 = bf16[192,4,256]{2,1,0:T(4,128)(2,1)} reshape(bf16[192,1024]{1,0:T(8,128)(2,1)} %get-tuple-element.26) | data formatting | bytes 786432 | tf_op jit(solution)/shard_map/reshape | solution.py:447
  153.7 1.0 copy.57
  154.8 1.4 fusion.22
  157.1 0.7 copy-done.29
  159.6 20.5 %return_and_norms.1 = (bf16[192,512]{1,0:T(8,128)(2,1)S(1)}, f32[2,192]{1,0:T(2,128)S(1)}, f32[8,1024]{1,0:T(8,128)S(1)}, bf16[3,2,512,1024]{3,2,1,0:T(8,128)(2,1)}, f32[3,512,256]{2,1,0:T(8,128)S(1)}) custom-call(bf16[512,288]{1,0:T(8,128)(2,1)S(1)} %bitcast.93, bf16[512,288]{1,0:T(8,128)(2,1)S(1)} %bitcast.94, bf16[512,288]{1,0:T(8,128)(2,1)S(1)} %bitcast.96, ...), custom_call_target="tpu_custom_call" | custom-call | tf_op jit(solution)/shard_map/return_and_norms/pallas_call | solution.py:341
  180.1 1.1 copy-done.21
  181.3 0.7 copy-done.25
  183.1 0.6 reshape.115
  183.8 1.6 copy.76
  185.4 7.0 %copy.77 = bf16[3,2,512,1024]{3,2,1,0:T(8,128)(2,1)} copy(bf16[3,2,512,1024]{3,2,1,0:T(8,128)(2,1)} %get-tuple-element.39) | data formatting | bytes 12582912
  192.4 1.1 copy.78
  (84 shorter events, 6.1 us)
Async XLA Ops:
  0.6 2.1 %copy-start = (bf16[512,1024]{1,0:T(8,128)(2,1)S(1)}, bf16[512,1024]{1,0:T(8,128)(2,1)}, u32[]{:S(2)}) copy-start(bf16[512,1024]{1,0:T(8,128)(2,1)} %param.17) | copy-start | bytes 3145732
  0.7 30.6 %copy-start.33 = (s32[2]{0:T(128)}, s32[2]{0:T(128)S(1)}, u32[]{:S(2)}) copy-start(s32[2]{0:T(128)S(1)} %iota_add_fusion) | copy-start | bytes 28
  29.7 5.2 %copy-start.1 = (bf16[4,192,512]{2,1,0:T(8,128)(2,1)S(1)}, bf16[4,192,512]{2,1,0:T(8,128)(2,1)}, u32[]{:S(2)}) copy-start(bf16[4,192,512]{2,1,0:T(8,128)(2,1)} %get-tuple-element.15.refs_4_) | copy-start | bytes 2359300
  30.6 0.6 copy-start.32
  32.0 4.3 %copy-start.26 = (pred[4,2,72,192]{3,2,0,1:T(8,128)(4,1)}, pred[4,2,72,192]{3,2,0,1:T(8,128)(4,1)S(1)}, u32[]{:S(2)}) copy-start(pred[4,2,72,192]{3,2,0,1:T(8,128)(4,1)S(1)} %fusion.16) | copy-start | bytes 331780
  33.4 7.5 %copy-start.4 = (bf16[4,72,512]{2,1,0:T(8,128)(2,1)}, bf16[4,72,512]{2,1,0:T(8,128)(2,1)S(1)}, u32[]{:S(2)}) copy-start(bf16[4,72,512]{2,1,0:T(8,128)(2,1)S(1)} %convolution_convert_fusion.1) | copy-start | bytes 884740
  34.9 6.0 %copy-start.6 = (bf16[4,72,512]{2,1,0:T(8,128)(2,1)}, bf16[4,72,512]{2,1,0:T(8,128)(2,1)S(1)}, u32[]{:S(2)}) copy-start(bf16[4,72,512]{2,1,0:T(8,128)(2,1)S(1)} %convolution_convert_fusion) | copy-start | bytes 884740
  35.2 6.6 %copy-start.8 = (bf16[4,72,512]{2,1,0:T(8,128)(2,1)}, bf16[4,72,512]{2,1,0:T(8,128)(2,1)S(1)}, u32[]{:S(2)}) copy-start(bf16[4,72,512]{2,1,0:T(8,128)(2,1)S(1)} %convolution_convert_fusion.2) | copy-start | bytes 884740
  35.2 6.6 %copy-start.2 = (bf16[4,192,512]{2,1,0:T(8,128)(2,1)S(1)}, bf16[4,192,512]{2,1,0:T(8,128)(2,1)}, u32[]{:S(2)}) copy-start(bf16[4,192,512]{2,1,0:T(8,128)(2,1)} %get-tuple-element.16.refs_5_) | copy-start | bytes 2359300
  43.3 1.0 copy-start.5
  44.2 1.0 copy-start.7
  45.2 1.0 copy-start.9
  46.2 1.0 copy-start.10
  47.1 0.9 copy-start.11
  48.1 0.9 copy-start.13
  49.0 1.6 copy-start.15
  50.6 1.0 copy-start.23
  51.6 0.9 copy-start.24
  52.6 83.4 %copy-start.27 = (pred[4,2,72,192]{3,2,0,1:T(8,128)(4,1)S(1)}, pred[4,2,72,192]{3,2,0,1:T(8,128)(4,1)}, u32[]{:S(2)}) copy-start(pred[4,2,72,192]{3,2,0,1:T(8,128)(4,1)} %copy-done.26) | copy-start | bytes 331780
  135.9 3.0 %copy-start.30 = (bf16[2,512,1024]{2,1,0:T(8,128)(2,1)S(1)}, bf16[2,512,1024]{2,1,0:T(8,128)(2,1)}, u32[]{:S(2)}) copy-start(bf16[2,512,1024]{2,1,0:T(8,128)(2,1)} %refs_7_.1) | copy-start | bytes 6291460
  139.0 2.5 %copy-start.16 = (bf16[2,512,1024]{2,1,0:T(8,128)(2,1)S(1)}, bf16[2,512,1024]{2,1,0:T(8,128)(2,1)}, u32[]{:S(2)}) copy-start(bf16[2,512,1024]{2,1,0:T(8,128)(2,1)} %refs_6_.1) | copy-start | bytes 6291460
  148.4 6.3 %copy-start.28 = (pred[4,2,72,192]{3,2,0,1:T(8,128)(4,1)S(1)}, pred[4,2,72,192]{3,2,0,1:T(8,128)(4,1)}, u32[]{:S(2)}) copy-start(pred[4,2,72,192]{3,2,0,1:T(8,128)(4,1)} %copy-done.26) | copy-start | bytes 331780
  150.6 5.6 %copy-start.12 = (bf16[512,256]{1,0:T(8,128)(2,1)S(1)}, bf16[512,256]{1,0:T(8,128)(2,1)}, u32[]{:S(2)}) copy-start(bf16[512,256]{1,0:T(8,128)(2,1)} %constant_dynamic-slice_fusion.2.refs_9_) | copy-start | bytes 786436
  154.7 1.9 copy-start.14
  156.2 2.3 %slice-start = ((s8[4915200]{0:T(1024)(128)(4,1)}), s8[4194304]{0:T(1024)(128)(4,1)S(1)}, s32[]{:S(2)}) async-start(s8[4915200]{0:T(1024)(128)(4,1)} %bitcast.74), calls=%async_computation | async-start | bytes 8388608
  156.6 1.1 copy-start.29
  156.6 1.2 copy-start.31
  156.6 2.2 %slice-start.1 = ((s8[4915200]{0:T(1024)(128)(4,1)}), s8[720896]{0:T(1024)(128)(4,1)S(1)}, s32[]{:S(2)}) async-start(s8[4915200]{0:T(1024)(128)(4,1)} %bitcast.74), calls=%async_computation.1 | async-start | bytes 1441792
  157.9 1.4 copy-start.3
  157.9 1.4 copy-start.17
  157.9 1.5 copy-start.18
  157.9 1.7 copy-start.19
  157.9 1.8 copy-start.20
  180.1 1.1 copy-start.21
  181.3 0.7 copy-start.25
  185.4 7.0 %copy-start.22 = (f32[3,512,256]{2,1,0:T(8,128)S(1)}, f32[3,512,256]{2,1,0:T(8,128)}, u32[]{:S(2)}) copy-start(f32[3,512,256]{2,1,0:T(8,128)} %copy-done.21) | copy-start | bytes 4718596

commit v3 on v2

--- a/solution.py
+++ b/solution.py
@@ -265,7 +265,7 @@
         ]
         + [pltpu.SemaphoreType.DMA((2, blocks // 4))] * 8,
         compiler_params=pltpu.CompilerParams(
-            collective_id=1, has_side_effects=True, vmem_limit_bytes=48 * 2**20
+            collective_id=1, has_side_effects=True, vmem_limit_bytes=30 * 2**20
         ),
         name="line_over_tp",
     )(*args)
@@ -299,11 +299,11 @@
     sq[...] = jnp.zeros_like(sq)
     hidden = eg_out.shape[3]
     part = sh_out.shape[2]
-    each = lhs[0][0].shape[1]
+    each = lhs[0][0].shape[0]
     deep = each // ROWS
     amount, size = tiles(hidden)
     for k, (block, right) in enumerate(((tokt, tg), (tokt, tu), (cott, ts))):
-        value = jnp.dot(block[...], right[...], preferred_element_type=F32)
+        value = mm(block[...], right[...], ((0,), (0,)))
         sh_out[k] = value
         sq[3 * local : 3 * local + 1, k * part : (k + 1) * part] = jnp.sum(value * value, axis=0, keepdims=True)
     for l in range(local):
@@ -313,7 +313,7 @@
                 cols = pl.ds(pl.multiple_of(i * size, size), size)
                 src = pl.ds(pl.multiple_of(k * hidden + i * size, size), size)
                 right = grads[l * deep : (l + 1) * deep, :, src].reshape(each, size)
-                value = jnp.dot(lhs[k // 2][l][...], right, preferred_element_type=F32)
+                value = mm(lhs[k // 2][l][...], right, ((0,), (0,)))
                 eg_out[k, l, :, cols] = value.astype(BF16)
                 sq[k * local + l : k * local + l + 1, cols] = jnp.sum(value * value, axis=0, keepdims=True)
                 return 0
@@ -329,13 +329,13 @@
     gate_out[...] = gate[me] + sum(rgate[s] for s in range(ne - 1))
     for copy in sums:
         copy.wait()
-    sq_out[...] = (sq[...] + sum(rsq[s] for s in range(nt - 1))) * (1.0 / (tokt.shape[0] * nt))
+    sq_out[...] = (sq[...] + sum(rsq[s] for s in range(nt - 1))) * (1.0 / (tokt.shape[1] * nt))
 
 
 def return_and_norms(xt, gt, tokt, cott, tg, tu, ts, grads, con, gate):
     ne, nt = lax.axis_size("ep"), lax.axis_size("tp")
     local = len(xt)
-    width, hidden, part = tokt.shape[0], (grads.shape[2] - 128) // 3, tg.shape[1]
+    width, hidden, part = tokt.shape[1], (grads.shape[2] - 128) // 3, tg.shape[1]
     sq_shape = (-(-(3 * local + 1) // 8) * 8, hidden)
     args = (*xt, *gt, tokt, cott, tg, tu, ts, grads, con, gate)
     return pl.pallas_call(
@@ -358,7 +358,7 @@
         + [pltpu.SemaphoreType.DMA((ne - 1,))] * 4
         + [pltpu.SemaphoreType.DMA((nt - 1,))] * 2,
         compiler_params=pltpu.CompilerParams(
-            collective_id=2, has_side_effects=True, vmem_limit_bytes=40 * 2**20
+            collective_id=2, has_side_effects=True, vmem_limit_bytes=24 * 2**20
         ),
         name="return_and_norms",
     )(*args)
@@ -460,10 +460,10 @@
     gate_con = jnp.sum(match * gate_tok[:, :, None], axis=1)
 
     token_grad, gate_out, squares, routed, shared = return_and_norms(
-        [a.T for a in xs],
-        [a.T for a in gs],
-        tok.reshape(groups * here, width).T,
-        cot.reshape(groups * here, width).T,
+        xs,
+        gs,
+        tok.reshape(groups * here, width),
+        cot.reshape(groups * here, width),
         tg,
         tu,
         ts,

time: 195 us -> 178 us (0.913)
  local copies, waits for them, and re-layouts: 45.3 us -> 35.5 us
  Pallas kernels: 127 us -> 121 us
    reshape x6 -> x0, local copies, waits for them, and re-layouts: 6.1 us -> none  [the longest x4 4.68 us: take(): jnp.einsum('gct,gtd->gcd', pick[:, l], rows, preferred_element_type=F32)]
    pallas_call x1, Pallas kernels: 82.2 us -> 77.7 us  [line_over_tp(): pl.pallas_call(functools.partial(line_kernel, n, len(xs)), out_shape=jax....]
    unnamed x75 -> x55, local copies, waits for them, and re-layouts: 23.7 us -> 19.9 us
where the time goes in v3:
time: 178 us; the launch traced here: 176 us
  Pallas kernels  121 us (68%)
  local copies, waits for them, and re-layouts  35.5 us (20%)
  matrix products  14.8 us (8%)
  other arithmetic  3.98 us (2%)
    pallas_call x1, Pallas kernels, line_over_tp(): pl.pallas_call(functools.partial(line_kernel, n, len(xs)), out_shape=jax....  77.7 us
    pallas_call x1, Pallas kernels, gather_over_ep(): pl.pallas_call(functools.partial(gather_kernel, n), out_shape=[jax.ShapeD...  24.3 us
    unnamed x55, local copies, waits for them, and re-layouts  19.9 us
    pallas_call x1, Pallas kernels, return_and_norms(): pl.pallas_call(functools.partial(return_kernel, ne, nt, local), out_shape...  19.1 us
    dot_general x7, matrix products, mm(): return lax.dot_general(a, b, (dims, ((), ())), preferred_element_type=F32)  9.29 us
    reshape x3, local copies, waits for them, and re-layouts, tall(): block.reshape(here, groups, part).transpose(1, 0, 2)  5.1 us
    transpose x3, local copies, waits for them, and re-layouts, tall(): block.reshape(here, groups, part).transpose(1, 0, 2)  3.91 us

profile of v3, /device:TPU:0, one launch (start us, length us, event | category | flops | bytes accessed | tf_op | source)
XLA Modules:
  0.0 176.4 jit_solution(17731116965691297051)
XLA Ops:
  0.7 0.8 convert_bitcast_fusion.1
  1.4 0.7 convert_bitcast_fusion
  2.1 0.6 pad_maximum_fusion.meta
  2.7 0.7 constant_dynamic-slice_fusion.2.refs_9_
  3.5 1.8 %constant_dynamic-slice_fusion = (bf16[512,256]{1,0:T(8,128)(2,1)S(1)}, bf16[512,256]{1,0:T(8,128)(2,1)}) fusion(bf16[512,1024]{1,0:T(8,128)(2,1)} %param.19, s32[]{:T(128)S(6)} %select_n.2, bf16[512,1024]{1,0:T(8,128)(2,1)} %param.18), kind=kLoop, calls=%fused_computation.52 | loop fusion | bytes 1048580 | tf_op jit(solution)/shard_map/dynamic_slice | solution.py:419
  5.2 24.3 %gather_over_ep.1 = (bf16[4,192,512]{2,1,0:T(8,128)(2,1)}, bf16[4,192,512]{2,1,0:T(8,128)(2,1)}, f32[4,4,192]{2,1,0:T(4,128)}) custom-call(bf16[192,512]{1,0:T(8,128)(2,1)} %tok.1, bf16[192,512]{1,0:T(8,128)(2,1)} %cot.1, f32[4,192]{1,0:T(4,128)} %pad_maximum_fusion.meta), custom_call_target="tpu_custom_call" | custom-call | tf_op jit(solution)/shard_map/gather_over_ep/pallas_call | solution.py:58
  29.6 0.8 slice_convert_fusion
  30.5 0.1 fusion.20
  30.7 0.3 multiply_reduce_fusion
  31.2 1.4 convolution_convert_fusion.1
  32.7 1.5 convolution_convert_fusion
  34.2 0.3 convolution_convert_fusion.2
  34.5 0.3 convolution_convert_fusion.3
  34.8 0.2 broadcast_in_dim.5.refs_12_
  35.0 1.6 copy-done.16
  36.6 1.6 copy-done.18
  38.2 77.7 %line_over_tp.1.refs_9_ = bf16[48,16,3200]{2,1,0:T(8,128)(2,1)S(1)} custom-call(bf16[288,512]{1,0:T(8,128)(2,1)S(1)} %bitcast.82, bf16[288,512]{1,0:T(8,128)(2,1)S(1)} %bitcast.80, bf16[288,512]{1,0:T(8,128)(2,1)S(1)} %bitcast.76, bf16[288,512]{1,0:T(8,128)(2,1)S(1)} %bitcast.78, bf16[4,192,512]{2,1,0:T(8,128)(2,1)S(1)} %copy-done.2, ...), custom_call_target="tpu_custom_call" | custom-call | tf_op jit(solution)/shard_map/line_over_tp/pallas_call | solution.py:255
  116.0 2.2 %copy-done.1 = bf16[48,16,3200]{2,1,0:T(8,128)(2,1)} copy-done((bf16[48,16,3200]{2,1,0:T(8,128)(2,1)}, bf16[48,16,3200]{2,1,0:T(8,128)(2,1)S(1)}, u32[]{:S(2)}) %copy-start.1) | copy-done | bytes 4915224
  118.2 0.1 slice_reduce_fusion
  118.4 0.2 fusion.17
  118.7 2.0 %fusion.3 = f32[288,512]{1,0:T(8,128)S(1)} fusion(bf16[2,512,1024]{2,1,0:T(8,128)(2,1)} %refs_6_.1, bf16[768,3200]{1,0:T(8,128)(2,1)} %bitcast.63), kind=kOutput, calls=%fused_computation.11 | convolution fusion | flops 301989888 | bytes 2228224 | tf_op jit(solution)/shard_map/dot_general | solution.py:368
  120.8 2.4 %fusion.1 = bf16[288,512]{1,0:T(8,128)(2,1)} fusion(f32[288,512]{1,0:T(8,128)S(1)} %fusion.3, bf16[2,512,1024]{2,1,0:T(8,128)(2,1)S(1)} %copy-done.19, bf16[768,3200]{1,0:T(8,128)(2,1)} %bitcast.64), kind=kOutput, calls=%fused_computation.5 | convolution fusion | flops 302284800 | bytes 2523136 | tf_op jit(solution)/shard_map/dot_general | solution.py:368
  123.3 1.6 fusion.6
  124.8 2.3 %fusion = bf16[288,512]{1,0:T(8,128)(2,1)} fusion(f32[288,512]{1,0:T(8,128)S(1)} %fusion.6, bf16[2,512,1024]{2,1,0:T(8,128)(2,1)S(1)} %copy-done.19, bf16[768,3200]{1,0:T(8,128)(2,1)} %bitcast.66), kind=kOutput, calls=%fused_computation.4 | convolution fusion | flops 302284800 | bytes 2523136 | tf_op jit(solution)/shard_map/dot_general | solution.py:368
  127.1 2.2 %fusion.28 = (bf16[192,1024]{1,0:T(8,128)(2,1)}, bf16[192,1024]{1,0:T(8,128)(2,1)S(1)}, bf16[192,1024]{1,0:T(8,128)(2,1)}) fusion(bf16[768,3200]{1,0:T(8,128)(2,1)} %bitcast.67), kind=kLoop, calls=%fused_computation.56 | loop fusion | bytes 2359296 | tf_op jit(solution)/shard_map/slice | solution.py:446
  129.3 2.0 %reshape.109 = bf16[192,4,256]{2,1,0:T(4,128)(2,1)} reshape(bf16[192,1024]{1,0:T(8,128)(2,1)} %get-tuple-element.24) | data formatting | bytes 786432 | tf_op jit(solution)/shard_map/reshape | solution.py:447
  131.4 1.8 %copy.31 = bf16[4,192,256]{2,1,0:T(8,128)(2,1)} copy(bf16[4,192,256]{2,0,1:T(4,128)(2,1)} %bitcast.87) | data formatting | bytes 786432 | tf_op jit(solution)/shard_map/transpose | solution.py:447
  133.2 1.0 reshape.107
  134.2 1.0 copy.30
  135.2 2.0 %reshape.105 = bf16[192,4,256]{2,1,0:T(4,128)(2,1)} reshape(bf16[192,1024]{1,0:T(8,128)(2,1)} %get-tuple-element.26) | data formatting | bytes 786432 | tf_op jit(solution)/shard_map/reshape | solution.py:447
  137.3 1.1 copy.29
  138.4 1.4 fusion.22
  139.8 0.4 fusion.29
  140.3 0.4 convolution_add_fusion
  140.7 0.7 copy-done.23
  141.4 0.4 add_convert_fusion.refs_10_
  141.9 0.2 slice-done
  142.1 0.3 slice-done.1
  142.4 0.2 copy-done.6
  142.9 19.1 %return_and_norms.1 = (bf16[192,512]{1,0:T(8,128)(2,1)S(1)}, f32[2,192]{1,0:T(2,128)S(1)}, f32[8,1024]{1,0:T(8,128)S(1)}, bf16[3,2,512,1024]{3,2,1,0:T(8,128)(2,1)S(1)}, f32[3,512,256]{2,1,0:T(8,128)S(1)}) custom-call(bf16[288,512]{1,0:T(8,128)(2,1)S(1)} %bitcast.83, bf16[288,512]{1,0:T(8,128)(2,1)S(1)} %bitcast.81, bf16[288,512]{1,0:T(8,128)(2,1)S(1)} %bitcast.77, ...), custom_call_target="tpu_custom_call" | custom-call | tf_op jit(solution)/shard_map/return_and_norms/pallas_call | solution.py:341
  162.0 2.7 %copy-done.4 = bf16[3,2,512,1024]{3,2,1,0:T(8,128)(2,1)} copy-done((bf16[3,2,512,1024]{3,2,1,0:T(8,128)(2,1)}, bf16[3,2,512,1024]{3,2,1,0:T(8,128)(2,1)S(1)}, u32[]{:S(2)}) %copy-start.4) | copy-done | bytes 6291480
  164.7 1.1 copy-done.21
  165.8 0.6 convert_bitcast_fusion.2
  166.4 0.6 reshape_squeeze.3
  167.0 0.6 reshape.115
  167.6 0.7 copy.48
  168.3 7.0 %copy.49 = bf16[3,2,512,1024]{3,2,1,0:T(8,128)(2,1)} copy(bf16[3,2,512,1024]{3,2,1,0:T(8,128)(2,1)} %copy-done.4) | data formatting | bytes 12582912
  175.3 1.1 copy.50
  (58 shorter events, 1.0 us)
Async XLA Ops:
  0.6 2.1 %copy-start = (bf16[512,1024]{1,0:T(8,128)(2,1)S(1)}, bf16[512,1024]{1,0:T(8,128)(2,1)}, u32[]{:S(2)}) copy-start(bf16[512,1024]{1,0:T(8,128)(2,1)} %param.17) | copy-start | bytes 3145732
  29.6 4.6 %copy-start.2 = (bf16[4,192,512]{2,1,0:T(8,128)(2,1)S(1)}, bf16[4,192,512]{2,1,0:T(8,128)(2,1)}, u32[]{:S(2)}) copy-start(bf16[4,192,512]{2,1,0:T(8,128)(2,1)} %get-tuple-element.15.refs_4_) | copy-start | bytes 2359300
  32.6 2.3 %copy-start.3 = (bf16[4,192,512]{2,1,0:T(8,128)(2,1)S(1)}, bf16[4,192,512]{2,1,0:T(8,128)(2,1)}, u32[]{:S(2)}) copy-start(bf16[4,192,512]{2,1,0:T(8,128)(2,1)} %get-tuple-element.16.refs_5_) | copy-start | bytes 2359300
  32.6 2.3 %copy-start.11 = (bf16[512,256]{1,0:T(8,128)(2,1)S(1)}, bf16[512,256]{1,0:T(8,128)(2,1)}, u32[]{:S(2)}) copy-start(bf16[512,256]{1,0:T(8,128)(2,1)} %constant_dynamic-slice_fusion.2.refs_9_) | copy-start | bytes 786436
  32.6 2.3 %copy-start.13 = (bf16[512,256]{1,0:T(8,128)(2,1)S(1)}, bf16[512,256]{1,0:T(8,128)(2,1)}, u32[]{:S(2)}) copy-start(bf16[512,256]{1,0:T(8,128)(2,1)} %get-tuple-element.30.refs_10_) | copy-start | bytes 786436
  32.7 2.3 %copy-start.15 = (bf16[2,512,1024]{2,1,0:T(8,128)(2,1)S(1)}, bf16[2,512,1024]{2,1,0:T(8,128)(2,1)}, u32[]{:S(2)}) copy-start(bf16[2,512,1024]{2,1,0:T(8,128)(2,1)} %refs_8_.1) | copy-start | bytes 6291460
  34.2 81.7 %copy-start.5 = (bf16[4,72,512]{2,1,0:T(8,128)(2,1)}, bf16[4,72,512]{2,1,0:T(8,128)(2,1)S(1)}, u32[]{:S(2)}) copy-start(bf16[4,72,512]{2,1,0:T(8,128)(2,1)S(1)} %convolution_convert_fusion) | copy-start | bytes 884740
  34.5 81.4 %copy-start.7 = (bf16[4,72,512]{2,1,0:T(8,128)(2,1)}, bf16[4,72,512]{2,1,0:T(8,128)(2,1)S(1)}, u32[]{:S(2)}) copy-start(bf16[4,72,512]{2,1,0:T(8,128)(2,1)S(1)} %convolution_convert_fusion.2) | copy-start | bytes 884740
  34.8 81.2 %copy-start.9 = (bf16[4,72,512]{2,1,0:T(8,128)(2,1)}, bf16[4,72,512]{2,1,0:T(8,128)(2,1)S(1)}, u32[]{:S(2)}) copy-start(bf16[4,72,512]{2,1,0:T(8,128)(2,1)S(1)} %convolution_convert_fusion.3) | copy-start | bytes 884740
  35.0 1.6 copy-start.16
  36.6 1.6 copy-start.18
  115.9 2.3 %copy-start.1 = (bf16[48,16,3200]{2,1,0:T(8,128)(2,1)}, bf16[48,16,3200]{2,1,0:T(8,128)(2,1)S(1)}, u32[]{:S(2)}) copy-start(bf16[48,16,3200]{2,1,0:T(8,128)(2,1)S(1)} %line_over_tp.1.refs_9_) | copy-start | bytes 14745604
  118.4 2.3 %copy-start.19 = (bf16[2,512,1024]{2,1,0:T(8,128)(2,1)S(1)}, bf16[2,512,1024]{2,1,0:T(8,128)(2,1)}, u32[]{:S(2)}) copy-start(bf16[2,512,1024]{2,1,0:T(8,128)(2,1)} %refs_7_.1) | copy-start | bytes 6291460
  120.8 2.5 %copy-start.17 = (bf16[2,512,1024]{2,1,0:T(8,128)(2,1)S(1)}, bf16[2,512,1024]{2,1,0:T(8,128)(2,1)}, u32[]{:S(2)}) copy-start(bf16[2,512,1024]{2,1,0:T(8,128)(2,1)} %refs_6_.1) | copy-start | bytes 6291460
  137.3 2.5 %copy-start.12 = (bf16[512,256]{1,0:T(8,128)(2,1)S(1)}, bf16[512,256]{1,0:T(8,128)(2,1)}, u32[]{:S(2)}) copy-start(bf16[512,256]{1,0:T(8,128)(2,1)} %constant_dynamic-slice_fusion.2.refs_9_) | copy-start | bytes 786436
  138.4 1.9 %copy-start.14 = (bf16[512,256]{1,0:T(8,128)(2,1)S(1)}, bf16[512,256]{1,0:T(8,128)(2,1)}, u32[]{:S(2)}) copy-start(bf16[512,256]{1,0:T(8,128)(2,1)} %get-tuple-element.30.refs_10_) | copy-start | bytes 786436
  139.8 2.3 %slice-start = ((s8[4915200]{0:T(1024)(128)(4,1)}), s8[4194304]{0:T(1024)(128)(4,1)S(1)}, s32[]{:S(2)}) async-start(s8[4915200]{0:T(1024)(128)(4,1)} %bitcast.68), calls=%async_computation | async-start | bytes 8388608
  140.2 1.2 copy-start.23
  140.2 2.1 %slice-start.1 = ((s8[4915200]{0:T(1024)(128)(4,1)}), s8[720896]{0:T(1024)(128)(4,1)S(1)}, s32[]{:S(2)}) async-start(s8[4915200]{0:T(1024)(128)(4,1)} %bitcast.68), calls=%async_computation.1 | async-start | bytes 1441792
  141.4 1.2 copy-start.6
  141.4 1.3 copy-start.8
  141.4 1.3 copy-start.10
  141.4 1.5 copy-start.20
  162.0 2.7 %copy-start.4 = (bf16[3,2,512,1024]{3,2,1,0:T(8,128)(2,1)}, bf16[3,2,512,1024]{3,2,1,0:T(8,128)(2,1)S(1)}, u32[]{:S(2)}) copy-start(bf16[3,2,512,1024]{3,2,1,0:T(8,128)(2,1)S(1)} %get-tuple-element.39) | copy-start | bytes 18874372
  164.7 1.1 copy-start.21
  168.3 7.0 %copy-start.22 = (f32[3,512,256]{2,1,0:T(8,128)S(1)}, f32[3,512,256]{2,1,0:T(8,128)}, u32[]{:S(2)}) copy-start(f32[3,512,256]{2,1,0:T(8,128)} %copy-done.21) | copy-start | bytes 4718596
